TPU v7x, 32 devices: a whole 2x2x4 slice. The times are simulated.
32 devices in a mesh: ep: 32 (over z, y, x, core).
Axes of the slice: x: 2, y: 2, z: 4, core: 2. Of those that a mesh axis runs over, the one named last changes fastest.
Arguments:
- tokens: bfloat16 [1536, 2048], P('ep'), may hold values from -6 to 6
- history_length: int32 [1536], P('ep'), may hold values from 1024 to 8192
- norm_gain: float32 [2048], replicated, may hold values from 0.1 to 1.9
- w_query: bfloat16 [2048, 512], replicated, may hold values from -0.125 to 0.125
- w_key: bfloat16 [2048, 512], replicated, may hold values from -0.125 to 0.125
- w_value: bfloat16 [2048, 512], replicated, may hold values from -0.125 to 0.125
- w_gate: bfloat16 [2048, 512], replicated, may hold values from -0.125 to 0.125
- decay_rate: float32 [8], replicated, may hold values from 0.003 to 0.7
- state: float32 [1536, 8, 64, 64], P('ep'), may hold values from -4 to 4
- head_gain: float32 [512], replicated, may hold values from 0.1 to 1.9
- w_out: bfloat16 [512, 2048], replicated, may hold values from -0.25 to 0.25
- moe_gain: float32 [2048], replicated, may hold values from 0.1 to 1.9
- route_weights: float32 [1536, 2], P('ep'), may hold values from 0.3 to 3
- expert_group: int32 [1536], P('ep'), may hold values from 0 to 3, as said below
- expert_inner: int32 [1536, 2], P('ep'), may hold values from 0 to 7, as said below
- expert_gate: bfloat16 [32, 2048, 256], P('ep'), may hold values from -0.125 to 0.125
- expert_up: bfloat16 [32, 2048, 256], P('ep'), may hold values from -0.125 to 0.125
- expert_down: bfloat16 [32, 256, 2048], P('ep'), may hold values from -0.375 to 0.375
Outputs:
- output: bfloat16 [1536, 2048], P('ep')
- new_state: float32 [1536, 8, 64, 64], P('ep')
Inputs may be any that keep to these rules, and one draw needn't show every extreme that they name: `expert_group`: together with expert_inner it names 2 different experts of one group for each token. `expert_inner`: the rows of one device name one expert at most 6 times; in every draw some expert is named exactly 6 times by the rows of every device.
All inputs are finite; a program needn't handle non-finite values.
Results may differ from a plain program's by a relative error of at most 0.02.
Values may be sent and summed in bfloat16 or wider, within the bound.
A program may use at most 128 MiB of HBM per device.

v0:
```python
import jax
import jax.numpy as jnp
from jax import lax
from jax.sharding import PartitionSpec as P

GROUPS = 4
TOP_K = 2


epsilon = 1e-06


def rotate(values, places):
    halfway = values.shape[-1] // 2
    inverse = 10000.0 ** (-jnp.arange(halfway, dtype=jnp.float32) / halfway)
    angles = places[:, None] * inverse[None, :]
    cosine = jnp.cos(angles)[:, None, :]
    sine_table = jnp.sin(angles)[:, None, :]
    first_half = values[..., :halfway]
    second = values[..., halfway:]
    return jnp.concatenate(
        [first_half * cosine - second * sine_table, first_half * sine_table + second * cosine],
        axis=-1,
    )


def rms_scale(values, gains):
    return values * lax.rsqrt(jnp.mean(values * values, axis=-1, keepdims=True) + epsilon) * gains


def retention_step(
    tokens,
    history_length,
    norm_gain,
    w_query,
    w_key,
    w_value,
    w_gate,
    decay_rate,
    state,
    head_gain,
    w_out,
    moe_gain,
):
    row_count = tokens.shape[0]
    head_count = decay_rate.shape[0]
    head_width = state.shape[-1]
    inputs = tokens.astype(jnp.float32)
    normed = rms_scale(inputs, norm_gain).astype(jnp.bfloat16)

    def project(weights):
        return jnp.dot(normed, weights, preferred_element_type=jnp.float32).astype(jnp.bfloat16)

    queries = project(w_query).reshape(row_count, head_count, head_width).astype(jnp.float32)
    keys_now = project(w_key).reshape(row_count, head_count, head_width).astype(jnp.float32)
    values_now = project(w_value).reshape(row_count, head_count, head_width).astype(jnp.float32)
    gating = project(w_gate).astype(jnp.float32)
    places = history_length.astype(jnp.float32)
    queries = rotate(queries, places)
    keys_now = rotate(keys_now, places) * head_width ** (-0.5)
    retain = jnp.exp(-decay_rate)
    new_state = (
        retain[None, :, None, None] * state + keys_now[:, :, :, None] * values_now[:, :, None, :]
    )
    reading = jnp.einsum("bhk,bhkv->bhv", queries, new_state, precision=lax.Precision.HIGHEST)
    reading = rms_scale(reading, head_gain.reshape(head_count, head_width))
    mixed_heads = (
        reading.reshape(row_count, head_count * head_width) * jax.nn.silu(gating)
    ).astype(jnp.bfloat16)
    mixed_tokens = (
        inputs + jnp.dot(mixed_heads, w_out, preferred_element_type=jnp.float32)
    ).astype(jnp.bfloat16)
    normed_moe = rms_scale(mixed_tokens.astype(jnp.float32), moe_gain).astype(jnp.bfloat16)
    return (mixed_tokens, normed_moe, new_state)


def expert_apply(row_block, gate_weight, up_weight, down_weight):
    gate_part = jnp.dot(row_block, gate_weight, preferred_element_type=jnp.float32)
    up_part = jnp.dot(row_block, up_weight, preferred_element_type=jnp.float32)
    hidden = (jax.nn.silu(gate_part) * up_part).astype(jnp.bfloat16)
    return jnp.dot(hidden, down_weight, preferred_element_type=jnp.float32).astype(jnp.bfloat16)


def slot_positions(flat_ids, experts):
    onehot = (flat_ids[:, None] == jnp.arange(experts, dtype=jnp.int32)[None, :]).astype(jnp.int32)
    earlier = jnp.cumsum(onehot, axis=0) - onehot
    return jnp.sum(earlier * onehot, axis=1)


def local(
    tokens,
    history_length,
    norm_gain,
    w_query,
    w_key,
    w_value,
    w_gate,
    decay_rate,
    state,
    head_gain,
    w_out,
    moe_gain,
    route_weights,
    expert_group,
    expert_inner,
    expert_gate,
    expert_up,
    expert_down,
):
    experts = lax.axis_size("ep")
    per_group = experts // GROUPS
    seq_count = tokens.shape[0]
    capacity = max(2, 4 * seq_count // experts)
    model_width = tokens.shape[1]
    expert_ids = expert_group[:, None] * per_group + expert_inner
    mixed_tokens, normed_moe, new_state = retention_step(
        tokens,
        history_length,
        norm_gain,
        w_query,
        w_key,
        w_value,
        w_gate,
        decay_rate,
        state,
        head_gain,
        w_out,
        moe_gain,
    )
    flat_ids = expert_ids.reshape(-1)
    target = flat_ids * capacity + slot_positions(flat_ids, experts)
    placement_table = (
        target[:, None] == jnp.arange(experts * capacity, dtype=jnp.int32)[None, :]
    ).astype(jnp.bfloat16)
    repeated = jnp.repeat(normed_moe, TOP_K, axis=0)
    outgoing = jnp.einsum(
        "rs,rd->sd", placement_table, repeated, preferred_element_type=jnp.float32
    )
    outgoing = outgoing.astype(jnp.bfloat16).reshape(experts, capacity, model_width)
    incoming = lax.all_to_all(outgoing, "ep", split_axis=0, concat_axis=0, tiled=True)
    flat_rows = incoming.reshape(-1, model_width)
    outputs = expert_apply(flat_rows, expert_gate[0], expert_up[0], expert_down[0]).reshape(
        incoming.shape
    )
    returned_rows = lax.all_to_all(outputs, "ep", split_axis=0, concat_axis=0, tiled=True)
    collected = jnp.einsum(
        "rs,sd->rd",
        placement_table,
        returned_rows.reshape(experts * capacity, model_width),
        preferred_element_type=jnp.float32,
    )
    collected = collected.reshape(-1, TOP_K, model_width)
    routed = jnp.sum(collected * route_weights[:, :, None], axis=1)
    output = (mixed_tokens.astype(jnp.float32) + routed).astype(jnp.bfloat16)
    return (output, new_state)


def solution(mesh):
    return jax.shard_map(
        local,
        mesh=mesh,
        in_specs=(
            P("ep", None),
            P("ep"),
            P(),
            P(),
            P(),
            P(),
            P(),
            P(),
            P("ep", None, None, None),
            P(),
            P(),
            P(),
            P("ep", None),
            P("ep"),
            P("ep", None),
            P("ep", None, None),
            P("ep", None, None),
            P("ep", None, None),
        ),
        out_specs=(P("ep", None), P("ep", None, None, None)),
        check_vma=False,
    )
```

profile of v0, /device:TPU:0, one launch (start us, length us, event | category | flops | bytes accessed | tf_op | source)
XLA Modules:
  0.0 116.0 jit_solution(12863362898902258698)
XLA Ops:
  0.6 0.0 copy-start
  0.6 0.0 copy-start.2
  0.7 0.0 copy-start.4
  0.7 0.8 broadcast_multiply_fusion
  1.5 0.7 convert_element_type.80
  2.2 0.7 negate_exponential_fusion
  2.8 1.1 fusion.13
  3.9 0.8 mul.244
  4.7 0.7 broadcast_add_fusion
  5.3 0.1 copy.29
  5.4 0.1 eq.50
  5.6 0.1 fusion.26
  5.7 0.1 reduce_window_sum.11
  5.8 0.2 select_reduce_fusion
  6.0 2.2 %fusion.6 = f32[48,512]{1,0:T(8,128)S(1)} fusion(bf16[2048,512]{1,0:T(8,128)(2,1)} %param.22, bf16[48,2048]{1,0:T(8,128)(2,1)} %param.18, f32[2048]{0:T(1024)} %param.20, f32[48]{0:T(128)S(1)} %add_rsqrt_fusion.2), kind=kOutput, calls=%fused_computation.15 | convolution fusion | flops 101105664 | bytes 2400448 | tf_op jit(solution)/shard_map/dot_general | solution.py:52
  8.2 0.1 reshape.175
  8.3 0.0 copy-done.2
  8.3 0.0 copy-done.4
  8.3 2.1 %fusion.5 = f32[48,512]{1,0:T(8,128)S(1)} fusion(bf16[2048,512]{1,0:T(8,128)(2,1)} %param.23, bf16[48,2048]{1,0:T(8,128)(2,1)S(1)} %copy-done.2, f32[2048]{0:T(1024)S(1)} %copy-done.4, f32[48]{0:T(128)S(1)} %add_rsqrt_fusion.2), kind=kOutput, calls=%fused_computation.13 | convolution fusion | flops 101105664 | bytes 2400448 | tf_op jit(solution)/shard_map/dot_general | solution.py:52
  10.5 0.1 reshape.176
  10.5 2.1 %fusion.7 = f32[48,512]{1,0:T(8,128)S(1)} fusion(bf16[2048,512]{1,0:T(8,128)(2,1)} %param.21, bf16[48,2048]{1,0:T(8,128)(2,1)S(1)} %copy-done.2, f32[2048]{0:T(1024)S(1)} %copy-done.4, f32[48]{0:T(128)S(1)} %add_rsqrt_fusion.2), kind=kOutput, calls=%fused_computation.17 | convolution fusion | flops 101105664 | bytes 2400448 | tf_op jit(solution)/shard_map/dot_general | solution.py:52
  12.7 0.1 reshape.174
  12.8 0.2 multiply_cosine_fusion
  12.9 0.2 multiply_subtract_fusion
  13.2 0.2 pad_maximum_fusion
  13.3 8.7 %multiply_add_fusion = f32[48,8,64,64]{3,2,1,0:T(8,128)S(1)} fusion(f32[48,8,64,64]{3,2,1,0:T(8,128)} %param.26, f32[48,8,64]{2,1,0:T(8,128)S(1)} %reshape.176, f32[48,8,64]{2,1,0:T(8,128)S(1)} %get-tuple-element.13, f32[8]{0:T(128)S(1)} %negate_exponential_fusion), kind=kLoop, calls=%fused_computation | loop fusion | flops 4718592 | bytes 12779552 | tf_op jit(solution)/shard_map/add | solution.py:63
  22.0 0.0 copy-start.1
  22.0 10.9 %fusion.37 = f32[48,8,1,64]{3,2,1,0:T(1,128)S(1)} fusion(f32[48,8,64,1]{2,3,1,0:T(1,128)S(1)} %bitcast.31, f32[48,8,64,64]{3,2,1,0:T(8,128)S(1)} %multiply_add_fusion), kind=kOutput, calls=%fused_computation.67 | convolution fusion | flops 18874368 | bytes 6488064 | tf_op jit(solution)/shard_map/bhk,bhkv->bhv/dot_general | solution.py:65
  32.9 0.0 copy-done.1
  32.9 0.1 multiply_reduce_fusion.1
  33.0 0.1 copy.27
  33.1 0.1 copy.28
  33.2 0.1 multiply_multiply_fusion
  33.3 0.1 reshape.168
  33.4 0.0 copy-done
  33.4 0.0 copy-start.5
  33.4 2.8 %multiply_reduce_fusion = (f32[48]{0:T(128)S(1)}, f32[48,2048]{1,0:T(8,128)S(1)}) fusion(bf16[512,2048]{1,0:T(8,128)(2,1)S(1)} %copy-done, f32[48,512]{1,0:T(8,128)S(1)} %reshape.168, bf16[2048,512]{1,0:T(8,128)(2,1)} %param.24, bf16[48,2048]{1,0:T(8,128)(2,1)S(1)} %copy-done.2, f32[2048]{0:T(1024)S(1)} %copy-done.4, f32[48]{0:T(128)S(1)} %add_rsqrt_fusion.2), kind=kOutput, calls=%fused_computation.29 | convolution fusion | flops 202506192 | bytes 4891008 | tf_op jit(solution)/shard_map/dot_general | solution.py:71
  36.2 0.0 copy-start.3
  36.3 0.0 copy-done.5
  36.3 0.1 multiply_convert_fusion
  36.4 0.2 broadcast_in_dim.2
  36.6 0.1 reshape.169
  36.8 0.2 copy-done.3
  37.0 1.4 %convolution_convert_fusion.1 = bf16[192,2048]{1,0:T(8,128)(2,1)} fusion(bf16[96,2048]{1,0:T(8,128)(2,1)S(1)} %reshape.169, s32[96]{0:T(128)S(1)} %multiply_add_fusion.4), kind=kOutput, calls=%fused_computation.2 | convolution fusion | flops 75909120 | bytes 1180032 | tf_op jit(solution)/shard_map/rs,rd->sd/dot_general | solution.py:136
  38.3 1.3 %reshape.170 = bf16[32,6,2048]{2,1,0:T(8,128)(2,1)S(1)} reshape(bf16[192,2048]{1,0:T(8,128)(2,1)} %convolution_convert_fusion.1) | data formatting | bytes 1572864 | tf_op jit(solution)/shard_map/reshape | solution.py:139
  39.7 33.4 %all_to_all.10 = bf16[32,6,2048]{2,1,0:T(8,128)(2,1)} all-to-all(bf16[32,6,2048]{2,1,0:T(8,128)(2,1)S(1)} %reshape.170), channel_id=1, replica_groups=mesh['ep'=32] {'ep'}, dimensions={0} | all-to-all | bytes 1572864 | tf_op jit(solution)/shard_map/all_to_all | solution.py:140
  73.1 1.4 %reshape.171 = bf16[192,2048]{1,0:T(8,128)(2,1)S(1)} reshape(bf16[32,6,2048]{2,1,0:T(8,128)(2,1)} %all_to_all.10) | data formatting | bytes 1572864 | tf_op jit(solution)/shard_map/reshape | solution.py:141
  74.5 1.6 %fusion.11 = f32[192,256]{1,0:T(8,128)S(1)} fusion(bf16[192,2048]{1,0:T(8,128)(2,1)S(1)} %reshape.171, bf16[1,2048,256]{2,1,0:T(8,128)(2,1)} %param.33), kind=kOutput, calls=%fused_computation.20 | convolution fusion | flops 201326592 | bytes 2031616 | tf_op jit(solution)/shard_map/dot_general | solution.py:78
  76.1 3.5 %convolution_convert_fusion = bf16[192,2048]{1,0:T(8,128)(2,1)} fusion(bf16[192,2048]{1,0:T(8,128)(2,1)S(1)} %reshape.171, bf16[1,256,2048]{2,1,0:T(8,128)(2,1)} %param.35, bf16[1,2048,256]{2,1,0:T(8,128)(2,1)} %param.34, f32[192,256]{1,0:T(8,128)S(1)} %fusion.11), kind=kOutput, calls=%fused_computation.1 | convolution fusion | flops 403341312 | bytes 3866624 | tf_op jit(solution)/shard_map/dot_general | solution.py:81
  79.6 0.0 copy-start.6
  79.6 2.2 %reshape.172 = bf16[32,6,2048]{2,1,0:T(8,128)(2,1)} reshape(bf16[192,2048]{1,0:T(8,128)(2,1)} %convolution_convert_fusion) | data formatting | bytes 1572864 | tf_op jit(solution)/shard_map/reshape | solution.py:142
  81.9 0.0 copy-start.7
  81.9 3.6 %all-to-all-start.1 = ((bf16[32,6,2048]{2,1,0:T(8,128)(2,1)}), bf16[32,6,2048]{2,1,0:T(8,128)(2,1)S(1)}, u32[]{:S(2)}, u32[]{:S(2)}) async-start(bf16[32,6,2048]{2,1,0:T(8,128)(2,1)} %reshape.172), calls=%async_computation.1 | async-start | bytes 2097152 | tf_op jit(solution)/shard_map/all_to_all | solution.py:145
  85.5 0.1 reduce_sum.50
  85.6 0.1 copy.30
  85.7 0.0 copy-done.6
  85.7 26.0 %all-to-all-done.1 = bf16[32,6,2048]{2,1,0:T(8,128)(2,1)S(1)} async-done(((bf16[32,6,2048]{2,1,0:T(8,128)(2,1)}), bf16[32,6,2048]{2,1,0:T(8,128)(2,1)S(1)}, u32[]{:S(2)}, u32[]{:S(2)}) %all-to-all-start.1) | async-done | bytes 786464 | tf_op jit(solution)/shard_map/all_to_all | solution.py:145
  111.7 1.1 reshape.179
  112.8 0.0 copy-done.7
  112.8 1.5 %fusion.2 = f32[48,2048]{1,0:T(8,128)S(1)} fusion(bf16[192,2048,1]{1,0,2:T(8,128)(2,1)} %reshape.179, f32[48,2]{0,1:T(2,128)S(1)} %copy-done.7, s32[48,2]{0,1:T(2,128)S(1)} %multiply_add_fusion.3), kind=kOutput, calls=%fused_computation.7 | convolution fusion | flops 75810816 | bytes 1180416 | tf_op jit(solution)/shard_map/rs,sd->rd/dot_general | solution.py:146
  114.3 1.7 %add_convert_fusion = bf16[48,2048]{1,0:T(8,128)(2,1)} fusion(f32[48,2048]{1,0:T(8,128)} %copy-done.3, f32[48,2048]{1,0:T(8,128)S(1)} %fusion.2), kind=kLoop, calls=%fused_computation.27 | loop fusion | flops 196608 | bytes 983040 | tf_op jit(solution)/shard_map/convert_element_type | solution.py:154
  (6 shorter events, 0.0 us)
Async XLA Ops:
  0.6 32.8 %copy-start = (bf16[512,2048]{1,0:T(8,128)(2,1)S(1)}, bf16[512,2048]{1,0:T(8,128)(2,1)}, u32[]{:S(2)}) copy-start(bf16[512,2048]{1,0:T(8,128)(2,1)} %param.28) | copy-start | bytes 6291460
  0.6 7.7 %copy-start.2 = (bf16[48,2048]{1,0:T(8,128)(2,1)S(1)}, bf16[48,2048]{1,0:T(8,128)(2,1)}, u32[]{:S(2)}) copy-start(bf16[48,2048]{1,0:T(8,128)(2,1)} %param.18) | copy-start | bytes 589828
  0.7 7.7 %copy-start.4 = (f32[2048]{0:T(1024)S(1)}, f32[2048]{0:T(1024)}, u32[]{:S(2)}) copy-start(f32[2048]{0:T(1024)} %param.20) | copy-start | bytes 24580
  22.0 10.9 %copy-start.1 = (f32[48,8,64,64]{3,2,1,0:T(8,128)}, f32[48,8,64,64]{3,2,1,0:T(8,128)S(1)}, u32[]{:S(2)}) copy-start(f32[48,8,64,64]{3,2,1,0:T(8,128)S(1)} %multiply_add_fusion) | copy-start | bytes 18874372
  33.4 2.8 %copy-start.5 = (f32[2048]{0:T(1024)S(1)}, f32[2048]{0:T(1024)}, u32[]{:S(2)}) copy-start(f32[2048]{0:T(1024)} %param.29) | copy-start | bytes 24580
  36.2 0.8 copy-start.3
  79.6 6.0 %copy-start.6 = (s32[48,2]{0,1:T(2,128)S(1)}, s32[48,2]{0,1:T(2,128)}, u32[]{:S(2)}) copy-start(s32[48,2]{0,1:T(2,128)} %param.32) | copy-start | bytes 1156
  81.9 31.0 %copy-start.7 = (f32[48,2]{0,1:T(2,128)S(1)}, f32[48,2]{0,1:T(2,128)}, u32[]{:S(2)}) copy-start(f32[48,2]{0,1:T(2,128)} %param.30) | copy-start | bytes 1156
  81.9 29.8 %all-to-all-start.1 = ((bf16[32,6,2048]{2,1,0:T(8,128)(2,1)}), bf16[32,6,2048]{2,1,0:T(8,128)(2,1)S(1)}, u32[]{:S(2)}, u32[]{:S(2)}) async-start(bf16[32,6,2048]{2,1,0:T(8,128)(2,1)} %reshape.172), calls=%async_computation.1 | async-start | bytes 2097152 | tf_op jit(solution)/shard_map/all_to_all | solution.py:145
where the time goes:
time: 117 us; the launch traced here: 116 us
  blocking collectives  33.4 us (29%)
  matrix products  28 us (24%)
  waiting for transfers between devices  26 us (22%)
  other arithmetic  15.6 us (13%)
  local copies, waits for them, and re-layouts  8.41 us (7%)
  starting transfers between devices  3.62 us (3%)
    all_to_all x1, blocking collectives, local(): lax.all_to_all(outgoing, 'ep', split_axis=0, concat_axis=0, tiled=True)  33.4 us
    all_to_all x1, waiting for transfers between devices, local(): lax.all_to_all(outputs, 'ep', split_axis=0, concat_axis=0, tiled=True)  26 us
    dot_general x1, matrix products, retention_step(): jnp.einsum('bhk,bhkv->bhv', queries, new_state, precision=lax.Precision.H...  10.9 us
    add x1, other arithmetic, retention_step(): retain[None, :, None, None] * state  8.66 us
    dot_general x3, matrix products, project(): jnp.dot(normed, weights, preferred_element_type=jnp.float32)  6.45 us
    all_to_all x1, starting transfers between devices, local(): lax.all_to_all(outputs, 'ep', split_axis=0, concat_axis=0, tiled=True)  3.62 us
    dot_general x1, matrix products, expert_apply(): jnp.dot(hidden, down_weight, preferred_element_type=jnp.float32)  3.5 us
    dot_general x1, matrix products, retention_step(): jnp.dot(mixed_heads, w_out, preferred_element_type=jnp.float32)  2.79 us
  transfers between devices with their start and end apart: 1, of which 1 were waited for; matrix products, arithmetic and copies ran while one was open for 0% of the time, Pallas kernels for 0%

commit v1 on v0

--- a/solution.py
+++ b/solution.py
@@ -1,6 +1,8 @@
 import jax
 import jax.numpy as jnp
 from jax import lax
+from jax.experimental import pallas as pl
+from jax.experimental.pallas import tpu as pltpu
 from jax.sharding import PartitionSpec as P
 
 GROUPS = 4
@@ -74,17 +76,275 @@
     return (mixed_tokens, normed_moe, new_state)
 
 
-def expert_apply(row_block, gate_weight, up_weight, down_weight):
-    gate_part = jnp.dot(row_block, gate_weight, preferred_element_type=jnp.float32)
-    up_part = jnp.dot(row_block, up_weight, preferred_element_type=jnp.float32)
+MESH = pl.DeviceIdType.MESH
+CHUNKS = 4
+
+
+def dot(a, b):
+    return jnp.dot(a, b, preferred_element_type=jnp.float32)
+
+
+def exchange_kernel(
+    per_group,
+    normed,
+    mixed,
+    place,
+    collect,
+    token_meta,
+    gate_hbm,
+    up_hbm,
+    down_hbm,
+    out,
+    gate_w,
+    up_w,
+    down_w,
+    meta_send,
+    meta_recv,
+    zsend,
+    zrecv,
+    dsend,
+    drecv,
+    osend,
+    orecv,
+    csend,
+    crecv,
+    load_sem,
+    meta_sems,
+    z_sems,
+    d_sems,
+    o_sems,
+    c_sems,
+):
+    device = lax.axis_index("ep")
+    group = device // per_group
+    inner = device % per_group
+    width = zsend.shape[-1]
+    group_rows = zsend.shape[2]
+    peer_rows = dsend.shape[2]
+    slots = GROUPS * group_rows
+    rows = per_group * peer_rows
+
+    def column_peer(step):
+        other = lax.rem(group + step, GROUPS)
+        return other, other * per_group + inner
+
+    def plane_peer(step):
+        other = lax.rem(inner + step, per_group)
+        return other, group * per_group + other
+
+    def column_copy(source, target, sems, chunk, step):
+        other, peer = column_peer(step)
+        return pltpu.make_async_remote_copy(
+            src_ref=source.at[chunk, other],
+            dst_ref=target.at[chunk, group],
+            send_sem=sems.at[0, chunk, step],
+            recv_sem=sems.at[1, chunk, step],
+            device_id=(peer,),
+            device_id_type=MESH,
+        )
+
+    def plane_copy(source, target, sems, chunk, step):
+        other, peer = plane_peer(step)
+        return pltpu.make_async_remote_copy(
+            src_ref=source.at[chunk, other],
+            dst_ref=target.at[chunk, inner],
+            send_sem=sems.at[0, chunk, step],
+            recv_sem=sems.at[1, chunk, step],
+            device_id=(peer,),
+            device_id_type=MESH,
+        )
+
+    def meta_copy(step):
+        other, peer = column_peer(step)
+        return pltpu.make_async_remote_copy(
+            src_ref=meta_send.at[other],
+            dst_ref=meta_recv.at[group],
+            send_sem=meta_sems.at[0, step],
+            recv_sem=meta_sems.at[1, step],
+            device_id=(peer,),
+            device_id_type=MESH,
+        )
+
+    def each_column(act):
+        for step in (2, 1, 3):
+            act(step)
+
+    def each_plane(act):
+        def body(step, carry):
+            act(step)
+            return carry
+
+        lax.fori_loop(1, per_group, body, 0)
+
+    loads = [
+        pltpu.make_async_copy(source, target, load_sem.at[place_index])
+        for place_index, (source, target) in enumerate(
+            ((gate_hbm, gate_w), (up_hbm, up_w), (down_hbm, down_w))
+        )
+    ]
+    for load in loads:
+        load.start()
+    barrier = pltpu.get_barrier_semaphore()
+
+    def greet_column(step):
+        pl.semaphore_signal(barrier, inc=1, device_id=(column_peer(step)[1],), device_id_type=MESH)
+
+    def greet_plane(step):
+        pl.semaphore_signal(barrier, inc=1, device_id=(plane_peer(step)[1],), device_id_type=MESH)
+
+    each_column(greet_column)
+    each_plane(greet_plane)
+    placing = place[...]
+    meta = dot(placing, token_meta[...]).astype(jnp.bfloat16)
+    meta_send[...] = meta.reshape(meta_send.shape)
+    for chunk in range(CHUNKS):
+        columns = slice(chunk * width, (chunk + 1) * width)
+        block = dot(placing, normed[:, columns]).astype(jnp.bfloat16)
+        zsend[chunk] = block.reshape(zsend.shape[1:])
+    pl.semaphore_wait(barrier, GROUPS - 1 + per_group - 1)
+    each_column(lambda step: meta_copy(step).start())
+    for chunk in range(CHUNKS):
+        each_column(lambda step: column_copy(zsend, zrecv, z_sems, chunk, step).start())
+    meta_recv[group] = meta_send[group]
+    for chunk in range(CHUNKS):
+        zrecv[chunk, group] = zsend[chunk, group]
+    each_column(lambda step: meta_copy(step).wait_recv())
+    meta = meta_recv[...].reshape(slots, meta_recv.shape[-1]).astype(jnp.float32)
+    row_ids = lax.broadcasted_iota(jnp.int32, (slots, rows), 1).astype(jnp.float32) + 1.0
+    first = (row_ids == meta[:, 0:1]).astype(jnp.float32)
+    second = (row_ids == meta[:, 1:2]).astype(jnp.float32)
+    spread = (first + second).astype(jnp.bfloat16)
+    weights = first * (meta[:, 2:3] + meta[:, 3:4]) + second * (meta[:, 4:5] + meta[:, 5:6])
+    weights_high = weights.astype(jnp.bfloat16)
+    weights_low = (weights - weights_high.astype(jnp.float32)).astype(jnp.bfloat16)
+    for chunk in range(CHUNKS):
+        each_column(lambda step: column_copy(zsend, zrecv, z_sems, chunk, step).wait_recv())
+        block = lax.dot_general(
+            spread,
+            zrecv[chunk].reshape(slots, width),
+            (((0,), (0,)), ((), ())),
+            preferred_element_type=jnp.float32,
+        ).astype(jnp.bfloat16)
+        dsend[chunk] = block.reshape(dsend.shape[1:])
+        each_plane(lambda step: plane_copy(dsend, drecv, d_sems, chunk, step).start())
+        drecv[chunk, inner] = dsend[chunk, inner]
+    loads[0].wait()
+    loads[1].wait()
+    loads[2].wait()
+    gate_part = jnp.zeros((rows, gate_w.shape[1]), jnp.float32)
+    up_part = jnp.zeros((rows, gate_w.shape[1]), jnp.float32)
+    for chunk in range(CHUNKS):
+        columns = slice(chunk * width, (chunk + 1) * width)
+        each_plane(lambda step: plane_copy(dsend, drecv, d_sems, chunk, step).wait_recv())
+        block = drecv[chunk].reshape(rows, width)
+        gate_part += dot(block, gate_w[columns, :])
+        up_part += dot(block, up_w[columns, :])
     hidden = (jax.nn.silu(gate_part) * up_part).astype(jnp.bfloat16)
-    return jnp.dot(hidden, down_weight, preferred_element_type=jnp.float32).astype(jnp.bfloat16)
-
-
-def slot_positions(flat_ids, experts):
-    onehot = (flat_ids[:, None] == jnp.arange(experts, dtype=jnp.int32)[None, :]).astype(jnp.int32)
-    earlier = jnp.cumsum(onehot, axis=0) - onehot
-    return jnp.sum(earlier * onehot, axis=1)
+    for chunk in range(CHUNKS):
+        columns = slice(chunk * width, (chunk + 1) * width)
+        block = dot(hidden, down_w[:, columns]).astype(jnp.bfloat16)
+        osend[chunk] = block.reshape(osend.shape[1:])
+        each_plane(lambda step: plane_copy(osend, orecv, o_sems, chunk, step).start())
+        orecv[chunk, inner] = osend[chunk, inner]
+    for chunk in range(CHUNKS):
+        each_plane(lambda step: plane_copy(osend, orecv, o_sems, chunk, step).wait_recv())
+        block = orecv[chunk].reshape(rows, width)
+        block = (dot(weights_high, block) + dot(weights_low, block)).astype(jnp.bfloat16)
+        csend[chunk] = block.reshape(csend.shape[1:])
+        each_column(lambda step: column_copy(csend, crecv, c_sems, chunk, step).start())
+        crecv[chunk, group] = csend[chunk, group]
+    collecting = collect[...]
+    for chunk in range(CHUNKS):
+        columns = slice(chunk * width, (chunk + 1) * width)
+        each_column(lambda step: column_copy(csend, crecv, c_sems, chunk, step).wait_recv())
+        block = dot(collecting, crecv[chunk].reshape(slots, width))
+        out[:, columns] = (mixed[:, columns].astype(jnp.float32) + block).astype(jnp.bfloat16)
+    each_column(lambda step: meta_copy(step).wait_send())
+
+    def drain(chunk, carry):
+        each_column(lambda step: column_copy(zsend, zrecv, z_sems, chunk, step).wait_send())
+        each_column(lambda step: column_copy(csend, crecv, c_sems, chunk, step).wait_send())
+        each_plane(lambda step: plane_copy(dsend, drecv, d_sems, chunk, step).wait_send())
+        each_plane(lambda step: plane_copy(osend, orecv, o_sems, chunk, step).wait_send())
+        return carry
+
+    lax.fori_loop(0, CHUNKS, drain, 0)
+
+
+def earlier_equal(ids):
+    count = ids.shape[0]
+    before = jnp.arange(count)[:, None] > jnp.arange(count)[None, :]
+    return jnp.sum((ids[:, None] == ids[None, :]) & before, axis=1).astype(jnp.int32)
+
+
+def routed_experts(
+    mixed_tokens, normed_moe, route_weights, expert_group, expert_inner, expert_gate, expert_up, expert_down
+):
+    experts = lax.axis_size("ep")
+    per_group = experts // GROUPS
+    seq_count, model_width = normed_moe.shape
+    capacity = max(2, 4 * seq_count // experts)
+    group_rows = -(-min(seq_count, per_group * capacity // TOP_K) // 8) * 8
+    peer_rows = GROUPS * capacity
+    width = model_width // CHUNKS
+    hidden_width = expert_gate.shape[-1]
+    slots = GROUPS * group_rows
+    my_group = lax.axis_index("ep") // per_group
+    expert_ids = expert_group[:, None] * per_group + expert_inner
+    expert_slot = earlier_equal(expert_ids.reshape(-1)).reshape(seq_count, TOP_K)
+    row_code = expert_inner * peer_rows + my_group * capacity + expert_slot + 1
+    group_slot = expert_group * group_rows + earlier_equal(expert_group)
+    slot_ids = jnp.arange(slots, dtype=jnp.int32)
+    place = (slot_ids[:, None] == group_slot[None, :]).astype(jnp.bfloat16)
+    collect = (group_slot[:, None] == slot_ids[None, :]).astype(jnp.bfloat16)
+    high = lax.reduce_precision(route_weights, 8, 7)
+    low = route_weights - high
+    token_meta = jnp.concatenate(
+        [row_code.astype(jnp.float32), high[:, :1], low[:, :1], high[:, 1:], low[:, 1:]], axis=1
+    )
+    token_meta = jnp.pad(token_meta, ((0, 0), (0, 128 - token_meta.shape[1]))).astype(jnp.bfloat16)
+    vmem = pl.BlockSpec(memory_space=pltpu.VMEM)
+    hbm = pl.BlockSpec(memory_space=pl.ANY)
+    bf16 = jnp.bfloat16
+    column_buffer = pltpu.VMEM((CHUNKS, GROUPS, group_rows, width), bf16)
+    plane_buffer = pltpu.VMEM((CHUNKS, per_group, peer_rows, width), bf16)
+    meta_buffer = pltpu.VMEM((GROUPS, group_rows, 128), bf16)
+    dma = pltpu.SemaphoreType.DMA
+
+    def kernel(*refs):
+        exchange_kernel(per_group, *refs)
+
+    return pl.pallas_call(
+        kernel,
+        name="experts",
+        out_shape=jax.ShapeDtypeStruct((seq_count, model_width), bf16),
+        in_specs=[vmem] * 5 + [hbm] * 3,
+        out_specs=vmem,
+        scratch_shapes=[
+            pltpu.VMEM((model_width, hidden_width), bf16),
+            pltpu.VMEM((model_width, hidden_width), bf16),
+            pltpu.VMEM((hidden_width, model_width), bf16),
+            meta_buffer,
+            meta_buffer,
+            column_buffer,
+            column_buffer,
+            plane_buffer,
+            plane_buffer,
+            plane_buffer,
+            plane_buffer,
+            column_buffer,
+            column_buffer,
+            dma((3,)),
+            dma((2, GROUPS)),
+            dma((2, CHUNKS, GROUPS)),
+            dma((2, CHUNKS, per_group)),
+            dma((2, CHUNKS, per_group)),
+            dma((2, CHUNKS, GROUPS)),
+        ],
+        compiler_params=pltpu.CompilerParams(
+            collective_id=0, has_side_effects=True, vmem_limit_bytes=48 * 1024 * 1024
+        ),
+    )(normed_moe, mixed_tokens, place, collect, token_meta, expert_gate, expert_up, expert_down)
 
 
 def local(
@@ -107,12 +367,6 @@
     expert_up,
     expert_down,
 ):
-    experts = lax.axis_size("ep")
-    per_group = experts // GROUPS
-    seq_count = tokens.shape[0]
-    capacity = max(2, 4 * seq_count // experts)
-    model_width = tokens.shape[1]
-    expert_ids = expert_group[:, None] * per_group + expert_inner
     mixed_tokens, normed_moe, new_state = retention_step(
         tokens,
         history_length,
@@ -127,31 +381,16 @@
         w_out,
         moe_gain,
     )
-    flat_ids = expert_ids.reshape(-1)
-    target = flat_ids * capacity + slot_positions(flat_ids, experts)
-    placement_table = (
-        target[:, None] == jnp.arange(experts * capacity, dtype=jnp.int32)[None, :]
-    ).astype(jnp.bfloat16)
-    repeated = jnp.repeat(normed_moe, TOP_K, axis=0)
-    outgoing = jnp.einsum(
-        "rs,rd->sd", placement_table, repeated, preferred_element_type=jnp.float32
-    )
-    outgoing = outgoing.astype(jnp.bfloat16).reshape(experts, capacity, model_width)
-    incoming = lax.all_to_all(outgoing, "ep", split_axis=0, concat_axis=0, tiled=True)
-    flat_rows = incoming.reshape(-1, model_width)
-    outputs = expert_apply(flat_rows, expert_gate[0], expert_up[0], expert_down[0]).reshape(
-        incoming.shape
-    )
-    returned_rows = lax.all_to_all(outputs, "ep", split_axis=0, concat_axis=0, tiled=True)
-    collected = jnp.einsum(
-        "rs,sd->rd",
-        placement_table,
-        returned_rows.reshape(experts * capacity, model_width),
-        preferred_element_type=jnp.float32,
-    )
-    collected = collected.reshape(-1, TOP_K, model_width)
-    routed = jnp.sum(collected * route_weights[:, :, None], axis=1)
-    output = (mixed_tokens.astype(jnp.float32) + routed).astype(jnp.bfloat16)
+    output = routed_experts(
+        mixed_tokens,
+        normed_moe,
+        route_weights,
+        expert_group,
+        expert_inner,
+        expert_gate[0],
+        expert_up[0],
+        expert_down[0],
+    )
     return (output, new_state)
 
 

time: 117 us -> 86.6 us (0.74)
  Pallas kernels: 0 us -> 38.9 us
  blocking collectives: 33.4 us -> 0 us
  waiting for transfers between devices: 26 us -> 0 us
  matrix products: 28 us -> 19.2 us
  starting transfers between devices: 3.62 us -> 0 us
  other arithmetic: 15.6 us -> 17.8 us
    pallas_call x0 -> x1, Pallas kernels: none -> 38.9 us  [routed_experts(): pl.pallas_call(kernel, name='experts', out_shape=jax.ShapeDtypeStruct((se...]
    all_to_all x1 -> x0, blocking collectives: 33.4 us -> none  [local(): lax.all_to_all(outgoing, 'ep', split_axis=0, concat_axis=0, tiled=True)]
    all_to_all x1 -> x0, waiting for transfers between devices: 26 us -> none  [local(): lax.all_to_all(outputs, 'ep', split_axis=0, concat_axis=0, tiled=True)]
    dot_general x4 -> x0, matrix products: 7.93 us -> none  [the longest x1 3.5 us: expert_apply(): jnp.dot(hidden, down_weight, preferred_element_type=jnp.float32)]
    reshape x5 -> x2, local copies, waits for them, and re-layouts: 6.22 us -> 1.55 us  [routed_experts(): earlier_equal(expert_ids.reshape(-1)).reshape(seq_count, TOP_K)]
    all_to_all x1 -> x0, starting transfers between devices: 3.62 us -> none  [local(): lax.all_to_all(outputs, 'ep', split_axis=0, concat_axis=0, tiled=True)]
    unnamed x16 -> x29, local copies, waits for them, and re-layouts: 0.26 us -> 3.47 us
    dot_general x3, matrix products: 6.45 us -> 4.85 us  [project(): jnp.dot(normed, weights, preferred_element_type=jnp.float32)]
  transfers between devices with their start and end apart: 1 -> 0, of which waited for: 1 -> 0; matrix products, arithmetic and copies ran while one was open for 0% -> 0% of each run, Pallas kernels for 0% -> 0%
where the time goes in v1:
time: 86.6 us; the launch traced here: 86 us
  Pallas kernels  38.9 us (45%)
  matrix products  19.2 us (22%)
  other arithmetic  17.8 us (21%)
  local copies, waits for them, and re-layouts  9.15 us (11%)
  between operations  0.9 us (1%)
    pallas_call x1, Pallas kernels, routed_experts(): pl.pallas_call(kernel, name='experts', out_shape=jax.ShapeDtypeStruct((se...  38.9 us
    dot_general x1, matrix products, retention_step(): jnp.einsum('bhk,bhkv->bhv', queries, new_state, precision=lax.Precision.H...  10.9 us
    add x1, other arithmetic, retention_step(): retain[None, :, None, None] * state  8.5 us
    dot_general x3, matrix products, project(): jnp.dot(normed, weights, preferred_element_type=jnp.float32)  4.85 us
    unnamed x29, local copies, waits for them, and re-layouts  3.47 us
    dot_general x1, matrix products, retention_step(): jnp.dot(mixed_heads, w_out, preferred_element_type=jnp.float32)  3.44 us

profile of v1, /device:TPU:0, one launch (start us, length us, event | category | flops | bytes accessed | tf_op | source)
XLA Modules:
  0.0 86.0 jit_solution(15950492894278129398)
XLA Ops:
  0.6 0.0 copy-start
  0.6 0.0 copy-start.5
  0.7 0.0 copy-start.8
  0.7 1.2 %fusion.8 = f32[48]{0:T(128)S(1)} fusion(bf16[48,2048]{1,0:T(8,128)(2,1)} %param.18), kind=kLoop, calls=%fused_computation.18 | loop fusion | flops 294864 | bytes 196800 | tf_op jit(solution)/shard_map/reduce_sum | solution.py:30
  1.9 0.0 copy-start.10
  1.9 0.0 copy-start.12
  1.9 2.2 %fusion.4 = f32[48,512]{1,0:T(8,128)S(1)} fusion(bf16[2048,512]{1,0:T(8,128)(2,1)} %param.21, bf16[48,2048]{1,0:T(8,128)(2,1)} %param.18, f32[2048]{0:T(1024)} %param.20, f32[48]{0:T(128)S(1)} %add_rsqrt_fusion.2), kind=kOutput, calls=%fused_computation.10 | convolution fusion | flops 101105664 | bytes 2400448 | tf_op jit(solution)/shard_map/dot_general | solution.py:54
  4.2 0.1 reshape.128
  4.3 0.0 copy-done.5
  4.3 0.0 copy-done.8
  4.3 2.1 %fusion.3 = f32[48,512]{1,0:T(8,128)S(1)} fusion(bf16[2048,512]{1,0:T(8,128)(2,1)} %param.22, bf16[48,2048]{1,0:T(8,128)(2,1)S(1)} %copy-done.5, f32[2048]{0:T(1024)S(1)} %copy-done.8, f32[48]{0:T(128)S(1)} %add_rsqrt_fusion.2), kind=kOutput, calls=%fused_computation.8 | convolution fusion | flops 101105664 | bytes 2400448 | tf_op jit(solution)/shard_map/dot_general | solution.py:54
  6.4 0.1 reshape.129
  6.5 0.0 copy-done.12
  6.5 0.0 copy-start.6
  6.5 0.2 multiply_cosine_fusion
  6.7 0.2 multiply_subtract_fusion
  7.0 0.0 copy-start.13
  7.0 0.9 pad_maximum_fusion
  7.8 0.0 copy-done.10
  7.8 0.3 copy-done.6
  8.1 0.5 fusion.2
  8.6 0.1 reshape.130
  8.7 0.0 copy-done.13
  8.7 0.0 copy-start.7
  8.7 8.5 %multiply_add_fusion = f32[48,8,64,64]{3,2,1,0:T(8,128)S(1)} fusion(f32[48,8,64,64]{3,2,1,0:T(8,128)} %param.26, f32[48,8,64]{2,1,0:T(8,128)S(1)} %reshape.130, f32[48,8,64]{2,1,0:T(8,128)S(1)} %get-tuple-element.21, f32[8]{0:T(128)S(1)} %negate_exponential_fusion), kind=kLoop, calls=%fused_computation | loop fusion | flops 4718592 | bytes 12779552 | tf_op jit(solution)/shard_map/add | solution.py:65
  17.3 0.0 copy-start.4
  17.3 0.0 copy-done.7
  17.3 0.0 copy-start.11
  17.3 10.9 %fusion.27 = f32[48,8,1,64]{3,2,1,0:T(1,128)S(1)} fusion(f32[48,8,64,1]{2,3,1,0:T(1,128)S(1)} %bitcast.20, f32[48,8,64,64]{3,2,1,0:T(8,128)S(1)} %multiply_add_fusion), kind=kOutput, calls=%fused_computation.58 | convolution fusion | flops 18874368 | bytes 6488064 | tf_op jit(solution)/shard_map/bhk,bhkv->bhv/dot_general | solution.py:67
  28.2 0.0 copy-done.4
  28.2 0.1 multiply_reduce_fusion
  28.3 0.1 copy.48
  28.4 0.1 copy.49
  28.5 0.0 copy-done.11
  28.5 0.1 mul.226
  28.5 0.1 multiply_multiply_fusion
  28.7 0.7 reshape.126
  29.4 0.0 copy-done
  29.4 0.0 copy-start.9
  29.4 3.4 %fusion.5 = (f32[48]{0:T(128)}, bf16[48,2048]{1,0:T(8,128)(2,1)S(1)}) fusion(bf16[512,2048]{1,0:T(8,128)(2,1)S(1)} %copy-done, f32[48,512]{1,0:T(8,128)} %reshape.126, bf16[2048,512]{1,0:T(8,128)(2,1)} %param.24, bf16[48,2048]{1,0:T(8,128)(2,1)S(1)} %copy-done.5, f32[2048]{0:T(1024)S(1)} %copy-done.8, f32[48]{0:T(128)} %copy-done.10), kind=kOutput, calls=%fused_computation.15 | convolution fusion | flops 202506192 | bytes 4694400 | tf_op jit(solution)/shard_map/dot_general | solution.py:73
  32.9 0.6 add_rsqrt_fusion.1
  33.5 0.0 copy-done.9
  33.5 0.1 fusion.7.refs_0_
  33.6 0.9 %convert_reduce_fusion.1 = s32[48]{0:T(128)S(1)} fusion(s32[48]{0:T(128)} %param.31), kind=kLoop, calls=%fused_computation.39 | loop fusion | flops 11472 | bytes 384 | tf_op jit(solution)/shard_map/reduce_sum | solution.py:277
  34.5 1.3 %broadcast_multiply_fusion = (s32[48]{0:T(128)S(1)}, s32[48]{0:T(128)}) fusion(s32[48]{0:T(128)} %param.31, s32[48]{0:T(128)S(1)} %convert_reduce_fusion.1), kind=kLoop, calls=%fused_computation.54 | loop fusion | flops 144 | bytes 768 | tf_op jit(solution)/shard_map/mul | solution.py:293
  35.8 0.7 broadcast_add_fusion
  36.4 0.7 copy.50
  37.1 0.9 eq.63
  38.0 0.2 convert_reduce_fusion
  38.2 0.7 reshape.127
  38.9 0.8 copy.51
  39.7 0.7 convert_convert_fusion
  40.4 0.7 fusion.16
  41.1 0.5 fusion.23
  41.6 0.7 concatenate.16
  42.3 0.1 copy.52
  42.4 0.7 fusion.12.refs_2_
  43.1 0.8 fusion.15.refs_3_
  43.9 0.0 copy-done.1
  43.9 0.0 copy-start.2
  43.9 1.2 %copy-done.2 = bf16[1,2048,256]{2,1,0:T(8,128)(2,1)S(1)} copy-done((bf16[1,2048,256]{2,1,0:T(8,128)(2,1)S(1)}, bf16[1,2048,256]{2,1,0:T(8,128)(2,1)}, u32[]{:S(2)}) %copy-start.2) | copy-done | bytes 1048600
  45.1 1.2 %copy-done.3 = bf16[1,256,2048]{2,1,0:T(8,128)(2,1)S(1)} copy-done((bf16[1,256,2048]{2,1,0:T(8,128)(2,1)S(1)}, bf16[1,256,2048]{2,1,0:T(8,128)(2,1)}, u32[]{:S(2)}) %copy-start.3) | copy-done | bytes 1048600
  46.3 38.9 %experts.1 = bf16[48,2048]{1,0:T(8,128)(2,1)S(1)} custom-call(bf16[48,2048]{1,0:T(8,128)(2,1)S(1)} %fusion.7.refs_0_, bf16[48,2048]{1,0:T(8,128)(2,1)S(1)} %get-tuple-element.19.refs_1_, bf16[96,48]{1,0:T(8,128)(2,1)S(1)} %fusion.12.refs_2_, bf16[48,96]{1,0:T(8,128)(2,1)S(1)} %fusion.15.refs_3_, bf16[48,128]{1,0:T(8,128)(2,1)S(1)} %pad.5.refs_4_, ...), custom_call_target="tpu_custom_call" | custom-call | tf_op jit(solution)/shard_map/experts/pallas_call | solution.py:317
  85.3 0.7 copy.56
  (8 shorter events, 0.0 us)
Async XLA Ops:
  0.6 28.8 %copy-start = (bf16[512,2048]{1,0:T(8,128)(2,1)S(1)}, bf16[512,2048]{1,0:T(8,128)(2,1)}, u32[]{:S(2)}) copy-start(bf16[512,2048]{1,0:T(8,128)(2,1)} %param.28) | copy-start | bytes 6291460
  0.6 3.6 %copy-start.5 = (bf16[48,2048]{1,0:T(8,128)(2,1)S(1)}, bf16[48,2048]{1,0:T(8,128)(2,1)}, u32[]{:S(2)}) copy-start(bf16[48,2048]{1,0:T(8,128)(2,1)} %param.18) | copy-start | bytes 589828
  0.7 3.6 %copy-start.8 = (f32[2048]{0:T(1024)S(1)}, f32[2048]{0:T(1024)}, u32[]{:S(2)}) copy-start(f32[2048]{0:T(1024)} %param.20) | copy-start | bytes 24580
  1.9 5.9 %copy-start.10 = (f32[48]{0:T(128)}, f32[48]{0:T(128)S(1)}, u32[]{:S(2)}) copy-start(f32[48]{0:T(128)S(1)} %add_rsqrt_fusion.2) | copy-start | bytes 580
  1.9 4.6 %copy-start.12 = (s32[48]{0:T(128)S(1)}, s32[48]{0:T(128)}, u32[]{:S(2)}) copy-start(s32[48]{0:T(128)} %param.19) | copy-start | bytes 580
  6.5 1.6 %copy-start.6 = (bf16[2048,512]{1,0:T(8,128)(2,1)S(1)}, bf16[2048,512]{1,0:T(8,128)(2,1)}, u32[]{:S(2)}) copy-start(bf16[2048,512]{1,0:T(8,128)(2,1)} %param.23) | copy-start | bytes 6291460
  7.0 1.8 %copy-start.13 = (f32[8]{0:T(128)S(1)}, f32[8]{0:T(128)}, u32[]{:S(2)}) copy-start(f32[8]{0:T(128)} %param.25) | copy-start | bytes 100
  8.7 8.5 %copy-start.7 = (f32[48,8,64]{2,1,0:T(8,128)S(1)}, f32[48,8,64]{2,1,0:T(8,128)}, u32[]{:S(2)}) copy-start(f32[48,8,64]{2,1,0:T(8,128)} %get-tuple-element.20) | copy-start | bytes 294916
  17.3 10.9 %copy-start.4 = (f32[48,8,64,64]{3,2,1,0:T(8,128)}, f32[48,8,64,64]{3,2,1,0:T(8,128)S(1)}, u32[]{:S(2)}) copy-start(f32[48,8,64,64]{3,2,1,0:T(8,128)S(1)} %multiply_add_fusion) | copy-start | bytes 18874372
  17.3 11.2 %copy-start.11 = (f32[512]{0:T(512)S(1)}, f32[512]{0:T(512)}, u32[]{:S(2)}) copy-start(f32[512]{0:T(512)} %param.27) | copy-start | bytes 6148
  29.4 4.0 %copy-start.9 = (f32[2048]{0:T(1024)S(1)}, f32[2048]{0:T(1024)}, u32[]{:S(2)}) copy-start(f32[2048]{0:T(1024)} %param.29) | copy-start | bytes 24580
  29.4 14.5 %copy-start.1 = (bf16[1,2048,256]{2,1,0:T(8,128)(2,1)S(1)}, bf16[1,2048,256]{2,1,0:T(8,128)(2,1)}, u32[]{:S(2)}) copy-start(bf16[1,2048,256]{2,1,0:T(8,128)(2,1)} %param.33) | copy-start | bytes 3145732
  43.9 1.2 %copy-start.2 = (bf16[1,2048,256]{2,1,0:T(8,128)(2,1)S(1)}, bf16[1,2048,256]{2,1,0:T(8,128)(2,1)}, u32[]{:S(2)}) copy-start(bf16[1,2048,256]{2,1,0:T(8,128)(2,1)} %param.34) | copy-start | bytes 3145732
  45.1 1.2 %copy-start.3 = (bf16[1,256,2048]{2,1,0:T(8,128)(2,1)S(1)}, bf16[1,256,2048]{2,1,0:T(8,128)(2,1)}, u32[]{:S(2)}) copy-start(bf16[1,256,2048]{2,1,0:T(8,128)(2,1)} %param.35) | copy-start | bytes 3145732

commit v2 on v1

--- a/solution.py
+++ b/solution.py
@@ -12,22 +12,154 @@
 epsilon = 1e-06
 
 
-def rotate(values, places):
-    halfway = values.shape[-1] // 2
-    inverse = 10000.0 ** (-jnp.arange(halfway, dtype=jnp.float32) / halfway)
-    angles = places[:, None] * inverse[None, :]
-    cosine = jnp.cos(angles)[:, None, :]
-    sine_table = jnp.sin(angles)[:, None, :]
-    first_half = values[..., :halfway]
-    second = values[..., halfway:]
-    return jnp.concatenate(
-        [first_half * cosine - second * sine_table, first_half * sine_table + second * cosine],
-        axis=-1,
+BLOCK = 8
+
+
+def dot(a, b):
+    return jnp.dot(a, b, preferred_element_type=jnp.float32)
+
+
+def rms(values, gains):
+    mean = jnp.mean(values * values, axis=-1, keepdims=True)
+    return values * lax.rsqrt(mean + epsilon) * gains
+
+
+def retention_kernel(
+    tokens,
+    cosine,
+    sine,
+    norm_gain,
+    decay_rate,
+    head_gain,
+    moe_gain,
+    query_hbm,
+    key_hbm,
+    value_hbm,
+    gate_hbm,
+    out_hbm,
+    state_hbm,
+    mixed_out,
+    normed_out,
+    new_state_hbm,
+    query_w,
+    key_w,
+    value_w,
+    gate_w,
+    out_w,
+    state,
+    query_columns,
+    key_columns,
+    value_heads,
+    reading,
+    weight_sem,
+    in_sem,
+    out_sem,
+):
+    seq_count = tokens.shape[0]
+    heads, head_width = state.shape[1], state.shape[-1]
+    half = head_width // 2
+    blocks = seq_count // BLOCK
+    weight_copies = [
+        pltpu.make_async_copy(source, target, weight_sem.at[index])
+        for index, (source, target) in enumerate(
+            (
+                (key_hbm, key_w),
+                (query_hbm, query_w),
+                (value_hbm, value_w),
+                (gate_hbm, gate_w),
+                (out_hbm, out_w),
+            )
+        )
+    ]
+
+    def state_in(block):
+        rows = pl.ds(block * BLOCK, BLOCK)
+        return pltpu.make_async_copy(state_hbm.at[rows], state.at[rows], in_sem.at[block])
+
+    def state_out(block):
+        rows = pl.ds(block * BLOCK, BLOCK)
+        return pltpu.make_async_copy(state.at[rows], new_state_hbm.at[rows], out_sem.at[block])
+
+    for copy in weight_copies[:3]:
+        copy.start()
+    for block in range(blocks):
+        state_in(block).start()
+    for copy in weight_copies[3:]:
+        copy.start()
+    inputs = tokens[...].astype(jnp.float32)
+    normed = rms(inputs, norm_gain[...]).astype(jnp.bfloat16)
+    cosines = jnp.concatenate([cosine[...]] * (2 * heads), axis=1)
+    sines = jnp.concatenate([-sine[...], sine[...]] * heads, axis=1)
+    lane = lax.broadcasted_iota(jnp.int32, cosines.shape, 1)
+    leading = lax.rem(lane, head_width) < half
+
+    def rounded(weights):
+        return dot(normed, weights[...]).astype(jnp.bfloat16).astype(jnp.float32)
+
+    def rotated(values):
+        partner = jnp.where(
+            leading, jnp.roll(values, -half, axis=1), jnp.roll(values, half, axis=1)
+        )
+        return values * cosines + partner * sines
+
+    weight_copies[0].wait()
+    keys = rotated(rounded(key_w)) * head_width ** (-0.5)
+    weight_copies[1].wait()
+    queries = rotated(rounded(query_w))
+    for block in range(blocks):
+        rows = slice(block * BLOCK, (block + 1) * BLOCK)
+        key_columns[block] = keys[rows].T
+        query_columns[block] = queries[rows].T
+    weight_copies[2].wait()
+    values = rounded(value_w)
+    for head in range(heads):
+        value_heads[head] = values[:, head * head_width : (head + 1) * head_width]
+    retain = [
+        jnp.exp(jnp.full((1, head_width), -decay_rate[head], jnp.float32)) for head in range(heads)
+    ]
+
+    def update(block, carry):
+        state_in(block).wait()
+        for head in range(heads):
+            span = slice(head * head_width, (head + 1) * head_width)
+            block_values = value_heads[head, pl.ds(block * BLOCK, BLOCK), :]
+            block_keys = key_columns[block, span, :]
+            block_queries = query_columns[block, span, :]
+            rows = []
+            for index in range(BLOCK):
+                sequence = block * BLOCK + index
+                fresh = (
+                    retain[head] * state[sequence, head]
+                    + block_keys[:, index : index + 1] * block_values[index : index + 1, :]
+                )
+                state[sequence, head] = fresh
+                rows.append(
+                    jnp.sum(block_queries[:, index : index + 1] * fresh, axis=0, keepdims=True)
+                )
+            reading[head, pl.ds(block * BLOCK, BLOCK), :] = jnp.concatenate(rows, axis=0)
+        state_out(block).start()
+        return carry
+
+    lax.fori_loop(0, blocks, update, 0)
+    weight_copies[3].wait()
+    gating = rounded(gate_w)
+    read = jnp.concatenate(
+        [
+            rms(
+                reading[head],
+                head_gain[:, head * head_width : (head + 1) * head_width],
+            )
+            for head in range(heads)
+        ],
+        axis=1,
     )
-
-
-def rms_scale(values, gains):
-    return values * lax.rsqrt(jnp.mean(values * values, axis=-1, keepdims=True) + epsilon) * gains
+    mixed_heads = (read * jax.nn.silu(gating)).astype(jnp.bfloat16)
+    weight_copies[4].wait()
+    mixed_tokens = (inputs + dot(mixed_heads, out_w[...])).astype(jnp.bfloat16)
+    mixed_out[...] = mixed_tokens
+    normed_out[...] = rms(mixed_tokens.astype(jnp.float32), moe_gain[...]).astype(jnp.bfloat16)
+    for block in range(blocks):
+        state_out(block).wait()
 
 
 def retention_step(
@@ -44,53 +176,66 @@
     w_out,
     moe_gain,
 ):
-    row_count = tokens.shape[0]
-    head_count = decay_rate.shape[0]
+    heads = decay_rate.shape[0]
+    seq_count, model_width = tokens.shape
     head_width = state.shape[-1]
-    inputs = tokens.astype(jnp.float32)
-    normed = rms_scale(inputs, norm_gain).astype(jnp.bfloat16)
-
-    def project(weights):
-        return jnp.dot(normed, weights, preferred_element_type=jnp.float32).astype(jnp.bfloat16)
-
-    queries = project(w_query).reshape(row_count, head_count, head_width).astype(jnp.float32)
-    keys_now = project(w_key).reshape(row_count, head_count, head_width).astype(jnp.float32)
-    values_now = project(w_value).reshape(row_count, head_count, head_width).astype(jnp.float32)
-    gating = project(w_gate).astype(jnp.float32)
-    places = history_length.astype(jnp.float32)
-    queries = rotate(queries, places)
-    keys_now = rotate(keys_now, places) * head_width ** (-0.5)
-    retain = jnp.exp(-decay_rate)
-    new_state = (
-        retain[None, :, None, None] * state + keys_now[:, :, :, None] * values_now[:, :, None, :]
+    half = head_width // 2
+    blocks = seq_count // BLOCK
+    inverse = 10000.0 ** (-jnp.arange(half, dtype=jnp.float32) / half)
+    angles = history_length.astype(jnp.float32)[:, None] * inverse[None, :]
+    vmem = pl.BlockSpec(memory_space=pltpu.VMEM)
+    smem = pl.BlockSpec(memory_space=pltpu.SMEM)
+    hbm = pl.BlockSpec(memory_space=pl.ANY)
+    dma = pltpu.SemaphoreType.DMA
+    f32 = jnp.float32
+    row_shape = jax.ShapeDtypeStruct((seq_count, model_width), jnp.bfloat16)
+    return pl.pallas_call(
+        retention_kernel,
+        name="retention",
+        out_shape=(row_shape, row_shape, jax.ShapeDtypeStruct(state.shape, f32)),
+        in_specs=[vmem] * 4 + [smem] + [vmem] * 2 + [hbm] * 6,
+        out_specs=(vmem, vmem, hbm),
+        scratch_shapes=[pltpu.VMEM(w_query.shape, jnp.bfloat16)] * 4
+        + [
+            pltpu.VMEM(w_out.shape, jnp.bfloat16),
+            pltpu.VMEM(state.shape, f32),
+            pltpu.VMEM((blocks, heads * head_width, BLOCK), f32),
+            pltpu.VMEM((blocks, heads * head_width, BLOCK), f32),
+            pltpu.VMEM((heads, seq_count, head_width), f32),
+            pltpu.VMEM((heads, seq_count, head_width), f32),
+            dma((5,)),
+            dma((blocks,)),
+            dma((blocks,)),
+        ],
+        compiler_params=pltpu.CompilerParams(vmem_limit_bytes=60 * 1024 * 1024),
+    )(
+        tokens,
+        jnp.cos(angles),
+        jnp.sin(angles),
+        norm_gain.reshape(1, -1),
+        decay_rate,
+        head_gain.reshape(1, -1),
+        moe_gain.reshape(1, -1),
+        w_query,
+        w_key,
+        w_value,
+        w_gate,
+        w_out,
+        state,
     )
-    reading = jnp.einsum("bhk,bhkv->bhv", queries, new_state, precision=lax.Precision.HIGHEST)
-    reading = rms_scale(reading, head_gain.reshape(head_count, head_width))
-    mixed_heads = (
-        reading.reshape(row_count, head_count * head_width) * jax.nn.silu(gating)
-    ).astype(jnp.bfloat16)
-    mixed_tokens = (
-        inputs + jnp.dot(mixed_heads, w_out, preferred_element_type=jnp.float32)
-    ).astype(jnp.bfloat16)
-    normed_moe = rms_scale(mixed_tokens.astype(jnp.float32), moe_gain).astype(jnp.bfloat16)
-    return (mixed_tokens, normed_moe, new_state)
 
 
 MESH = pl.DeviceIdType.MESH
 CHUNKS = 4
-
-
-def dot(a, b):
-    return jnp.dot(a, b, preferred_element_type=jnp.float32)
 
 
 def exchange_kernel(
     per_group,
     normed,
     mixed,
-    place,
-    collect,
-    token_meta,
+    expert_group,
+    expert_inner,
+    route_weights,
     gate_hbm,
     up_hbm,
     down_hbm,
@@ -194,8 +339,42 @@
 
     each_column(greet_column)
     each_plane(greet_plane)
-    placing = place[...]
-    meta = dot(placing, token_meta[...]).astype(jnp.bfloat16)
+    seq_count = normed.shape[0]
+    group_row = expert_group[...].astype(jnp.float32)
+    inner_rows = [expert_inner[choice : choice + 1, :].astype(jnp.float32) for choice in (0, 1)]
+    square = (seq_count, seq_count)
+    above = lax.broadcasted_iota(jnp.int32, square, 0)
+    across = lax.broadcasted_iota(jnp.int32, square, 1)
+
+    def column(row):
+        return jnp.sum(jnp.where(above == across, row, 0.0), axis=1, keepdims=True)
+
+    def earlier(columns, row):
+        matched = sum((values == row).astype(jnp.float32) for values in columns)
+        return jnp.sum(jnp.where(above < across, matched, 0.0), axis=0, keepdims=True)
+
+    group_slot = group_row * group_rows + earlier([column(group_row)], group_row)
+    expert_rows = [group_row * per_group + row for row in inner_rows]
+    expert_columns = [column(row) for row in expert_rows]
+    capacity = peer_rows // GROUPS
+    own_rows = (group * capacity + 1).astype(jnp.float32)
+    lanes = []
+    for choice in (0, 1):
+        slot = earlier(expert_columns, expert_rows[choice])
+        lanes.append(column(inner_rows[choice] * peer_rows + own_rows + slot))
+    for choice in (0, 1):
+        weight = column(route_weights[choice : choice + 1, :])
+        high = weight.astype(jnp.bfloat16).astype(jnp.float32)
+        lanes += [high, weight - high]
+    lane = lax.broadcasted_iota(jnp.int32, (seq_count, meta_send.shape[-1]), 1)
+    token_meta = jnp.zeros(lane.shape, jnp.float32)
+    for index, value in enumerate(lanes):
+        token_meta = jnp.where(lane == index, value, token_meta)
+    slot_above = lax.broadcasted_iota(jnp.int32, (slots, seq_count), 0).astype(jnp.float32)
+    slot_across = lax.broadcasted_iota(jnp.int32, (seq_count, slots), 1).astype(jnp.float32)
+    placing = (slot_above == group_slot).astype(jnp.float32).astype(jnp.bfloat16)
+    collecting = (slot_across == column(group_slot)).astype(jnp.float32).astype(jnp.bfloat16)
+    meta = dot(placing, token_meta.astype(jnp.bfloat16)).astype(jnp.bfloat16)
     meta_send[...] = meta.reshape(meta_send.shape)
     for chunk in range(CHUNKS):
         columns = slice(chunk * width, (chunk + 1) * width)
@@ -253,7 +432,6 @@
         csend[chunk] = block.reshape(csend.shape[1:])
         each_column(lambda step: column_copy(csend, crecv, c_sems, chunk, step).start())
         crecv[chunk, group] = csend[chunk, group]
-    collecting = collect[...]
     for chunk in range(CHUNKS):
         columns = slice(chunk * width, (chunk + 1) * width)
         each_column(lambda step: column_copy(csend, crecv, c_sems, chunk, step).wait_recv())
@@ -269,12 +447,6 @@
         return carry
 
     lax.fori_loop(0, CHUNKS, drain, 0)
-
-
-def earlier_equal(ids):
-    count = ids.shape[0]
-    before = jnp.arange(count)[:, None] > jnp.arange(count)[None, :]
-    return jnp.sum((ids[:, None] == ids[None, :]) & before, axis=1).astype(jnp.int32)
 
 
 def routed_experts(
@@ -289,20 +461,6 @@
     width = model_width // CHUNKS
     hidden_width = expert_gate.shape[-1]
     slots = GROUPS * group_rows
-    my_group = lax.axis_index("ep") // per_group
-    expert_ids = expert_group[:, None] * per_group + expert_inner
-    expert_slot = earlier_equal(expert_ids.reshape(-1)).reshape(seq_count, TOP_K)
-    row_code = expert_inner * peer_rows + my_group * capacity + expert_slot + 1
-    group_slot = expert_group * group_rows + earlier_equal(expert_group)
-    slot_ids = jnp.arange(slots, dtype=jnp.int32)
-    place = (slot_ids[:, None] == group_slot[None, :]).astype(jnp.bfloat16)
-    collect = (group_slot[:, None] == slot_ids[None, :]).astype(jnp.bfloat16)
-    high = lax.reduce_precision(route_weights, 8, 7)
-    low = route_weights - high
-    token_meta = jnp.concatenate(
-        [row_code.astype(jnp.float32), high[:, :1], low[:, :1], high[:, 1:], low[:, 1:]], axis=1
-    )
-    token_meta = jnp.pad(token_meta, ((0, 0), (0, 128 - token_meta.shape[1]))).astype(jnp.bfloat16)
     vmem = pl.BlockSpec(memory_space=pltpu.VMEM)
     hbm = pl.BlockSpec(memory_space=pl.ANY)
     bf16 = jnp.bfloat16
@@ -342,9 +500,18 @@
             dma((2, CHUNKS, GROUPS)),
         ],
         compiler_params=pltpu.CompilerParams(
-            collective_id=0, has_side_effects=True, vmem_limit_bytes=48 * 1024 * 1024
+            collective_id=0, has_side_effects=True, vmem_limit_bytes=60 * 1024 * 1024
         ),
-    )(normed_moe, mixed_tokens, place, collect, token_meta, expert_gate, expert_up, expert_down)
+    )(
+        normed_moe,
+        mixed_tokens,
+        expert_group.reshape(1, -1),
+        expert_inner.T,
+        route_weights.T,
+        expert_gate,
+        expert_up,
+        expert_down,
+    )
 
 
 def local(

time: 86.6 us -> 60.5 us (0.70)
  matrix products: 19.2 us -> 0 us
  Pallas kernels: 38.9 us -> 56.6 us
  other arithmetic: 17.8 us -> 1.47 us
  local copies, waits for them, and re-layouts: 9.15 us -> 1.62 us
    dot_general x5 -> x0, matrix products: 19.2 us -> none  [the longest x1 10.9 us: retention_step(): jnp.einsum('bhk,bhkv->bhv', queries, new_state, precision=lax.Precision.H...]
    pallas_call x0 -> x1, Pallas kernels: none -> 16 us  [retention_step(): pl.pallas_call(retention_kernel, name='retention', out_shape=(row_shape,...]
    add x2 -> x0, other arithmetic: 9.19 us -> none  [the longest x1 8.5 us: retention_step(): retain[None, :, None, None] * state]
    reduce_sum x4 -> x0, other arithmetic: 2.43 us -> none  [the longest x2 1.35 us: rms_scale(): jnp.mean(values * values, axis=-1, keepdims=True) + epsilon]
    reshape x3 -> x0, local copies, waits for them, and re-layouts: 2.3 us -> none  [the longest x2 1.55 us: routed_experts(): earlier_equal(expert_ids.reshape(-1)).reshape(seq_count, TOP_K)]
    unnamed x29 -> x1, local copies, waits for them, and re-layouts: 3.47 us -> 1.62 us
    pallas_call x1, Pallas kernels: 38.9 us -> 40.6 us  [routed_experts(): pl.pallas_call(kernel, name='experts', out_shape=jax.ShapeDtypeStruct((se...]
    mul x2 -> x0, other arithmetic: 1.38 us -> none  [the longest x1 1.26 us: routed_experts(): expert_ids = expert_group[:, None] * per_group + expert_inner]
where the time goes in v2:
time: 60.5 us; the launch traced here: 60.3 us
  Pallas kernels  56.6 us (94%)
  local copies, waits for them, and re-layouts  1.62 us (3%)
  other arithmetic  1.47 us (2%)
  between operations  0.65 us (1%)
    pallas_call x1, Pallas kernels, routed_experts(): pl.pallas_call(kernel, name='experts', out_shape=jax.ShapeDtypeStruct((se...  40.6 us
    pallas_call x1, Pallas kernels, retention_step(): pl.pallas_call(retention_kernel, name='retention', out_shape=(row_shape,...  16 us
    unnamed x1, local copies, waits for them, and re-layouts  1.62 us

profile of v2, /device:TPU:0, one launch (start us, length us, event | category | flops | bytes accessed | tf_op | source)
XLA Modules:
  0.0 60.3 jit_solution(8575089751403197065)
XLA Ops:
  0.6 0.7 %convert_element_type.3 = f32[48]{0:T(128)S(1)} convert(s32[48]{0:T(128)} %param.19) | non-fusion elementwise | flops 48 | bytes 384 | tf_op jit(solution)/shard_map/convert_element_type | solution.py:185
  1.3 0.8 %multiply_sine_fusion = (f32[48,32]{1,0:T(8,128)}, f32[48,32]{1,0:T(8,128)}) fusion(f32[32]{0:T(128)S(1)} %multiply_power_fusion, f32[48]{0:T(128)S(1)} %convert_element_type.3), kind=kLoop, calls=%fused_computation | loop fusion | flops 1536 | bytes 12608 | tf_op jit(solution)/shard_map/sin | solution.py:214
  2.1 16.0 %retention.1 = (bf16[48,2048]{1,0:T(8,128)(2,1)}, bf16[48,2048]{1,0:T(8,128)(2,1)}, f32[48,8,64,64]{3,2,1,0:T(8,128)}) custom-call(bf16[48,2048]{1,0:T(8,128)(2,1)} %tokens.1, f32[48,32]{1,0:T(8,128)} %get-tuple-element.9.cosine, f32[48,32]{1,0:T(8,128)} %get-tuple-element.8.sine, f32[1,2048]{1,0:T(1,128)} %bitcast.12, f32[8]{0:T(128)} %decay_rate.1, ...), custom_call_target="tpu_custom_call" | custom-call | tf_op jit(solution)/shard_map/retention/pallas_call | solution.py:192
  18.1 40.6 %experts.1 = bf16[48,2048]{1,0:T(8,128)(2,1)} custom-call(bf16[48,2048]{1,0:T(8,128)(2,1)} %get-tuple-element.5.refs_0_, bf16[48,2048]{1,0:T(8,128)(2,1)} %get-tuple-element.6.refs_1_, s32[1,48]{1,0:T(1,128)} %bitcast.17, s32[2,48]{1,0:T(2,128)} %bitcast.15, f32[2,48]{1,0:T(2,128)} %bitcast.16, bf16[2048,256]{1,0:T(8,128)(2,1)} %bitcast.9, ...), custom_call_target="tpu_custom_call" | custom-call | tf_op jit(solution)/shard_map/experts/pallas_call | solution.py:475
  58.7 1.6 %copy.21 = bf16[48,2048]{1,0:T(8,128)(2,1)} copy(bf16[48,2048]{1,0:T(8,128)(2,1)} %experts.1) | data formatting | bytes 393216
  (1 shorter events, 0.0 us)

commit v3 on v2

--- a/solution.py
+++ b/solution.py
@@ -1,5 +1,6 @@
 import jax
 import jax.numpy as jnp
+import numpy as np
 from jax import lax
 from jax.experimental import pallas as pl
 from jax.experimental.pallas import tpu as pltpu
@@ -26,12 +27,11 @@
 
 def retention_kernel(
     tokens,
-    cosine,
-    sine,
+    history_length,
+    inverse,
     norm_gain,
     decay_rate,
     head_gain,
-    moe_gain,
     query_hbm,
     key_hbm,
     value_hbm,
@@ -39,7 +39,6 @@
     out_hbm,
     state_hbm,
     mixed_out,
-    normed_out,
     new_state_hbm,
     query_w,
     key_w,
@@ -88,8 +87,15 @@
         copy.start()
     inputs = tokens[...].astype(jnp.float32)
     normed = rms(inputs, norm_gain[...]).astype(jnp.bfloat16)
-    cosines = jnp.concatenate([cosine[...]] * (2 * heads), axis=1)
-    sines = jnp.concatenate([-sine[...], sine[...]] * heads, axis=1)
+    square = (seq_count, seq_count)
+    above = lax.broadcasted_iota(jnp.int32, square, 0)
+    across = lax.broadcasted_iota(jnp.int32, square, 1)
+    places = history_length[...].astype(jnp.float32)
+    places = jnp.sum(jnp.where(above == across, places, 0.0), axis=1, keepdims=True)
+    angles = places * inverse[...]
+    cosine, sine = jnp.cos(angles), jnp.sin(angles)
+    cosines = jnp.concatenate([cosine] * (2 * heads), axis=1)
+    sines = jnp.concatenate([-sine, sine] * heads, axis=1)
     lane = lax.broadcasted_iota(jnp.int32, cosines.shape, 1)
     leading = lax.rem(lane, head_width) < half
 
@@ -155,9 +161,7 @@
     )
     mixed_heads = (read * jax.nn.silu(gating)).astype(jnp.bfloat16)
     weight_copies[4].wait()
-    mixed_tokens = (inputs + dot(mixed_heads, out_w[...])).astype(jnp.bfloat16)
-    mixed_out[...] = mixed_tokens
-    normed_out[...] = rms(mixed_tokens.astype(jnp.float32), moe_gain[...]).astype(jnp.bfloat16)
+    mixed_out[...] = (inputs + dot(mixed_heads, out_w[...])).astype(jnp.bfloat16)
     for block in range(blocks):
         state_out(block).wait()
 
@@ -174,15 +178,13 @@
     state,
     head_gain,
     w_out,
-    moe_gain,
 ):
     heads = decay_rate.shape[0]
     seq_count, model_width = tokens.shape
     head_width = state.shape[-1]
     half = head_width // 2
     blocks = seq_count // BLOCK
-    inverse = 10000.0 ** (-jnp.arange(half, dtype=jnp.float32) / half)
-    angles = history_length.astype(jnp.float32)[:, None] * inverse[None, :]
+    inverse = (10000.0 ** (-np.arange(half) / half)).astype(np.float32)
     vmem = pl.BlockSpec(memory_space=pltpu.VMEM)
     smem = pl.BlockSpec(memory_space=pltpu.SMEM)
     hbm = pl.BlockSpec(memory_space=pl.ANY)
@@ -192,9 +194,9 @@
     return pl.pallas_call(
         retention_kernel,
         name="retention",
-        out_shape=(row_shape, row_shape, jax.ShapeDtypeStruct(state.shape, f32)),
-        in_specs=[vmem] * 4 + [smem] + [vmem] * 2 + [hbm] * 6,
-        out_specs=(vmem, vmem, hbm),
+        out_shape=(row_shape, jax.ShapeDtypeStruct(state.shape, f32)),
+        in_specs=[vmem] * 4 + [smem, vmem] + [hbm] * 6,
+        out_specs=(vmem, hbm),
         scratch_shapes=[pltpu.VMEM(w_query.shape, jnp.bfloat16)] * 4
         + [
             pltpu.VMEM(w_out.shape, jnp.bfloat16),
@@ -210,12 +212,11 @@
         compiler_params=pltpu.CompilerParams(vmem_limit_bytes=60 * 1024 * 1024),
     )(
         tokens,
-        jnp.cos(angles),
-        jnp.sin(angles),
+        history_length.reshape(1, -1),
+        inverse.reshape(1, -1),
         norm_gain.reshape(1, -1),
         decay_rate,
         head_gain.reshape(1, -1),
-        moe_gain.reshape(1, -1),
         w_query,
         w_key,
         w_value,
@@ -226,12 +227,12 @@
 
 
 MESH = pl.DeviceIdType.MESH
-CHUNKS = 4
+STAGES = GROUPS
 
 
 def exchange_kernel(
     per_group,
-    normed,
+    moe_gain,
     mixed,
     expert_group,
     expert_inner,
@@ -264,7 +265,7 @@
     group = device // per_group
     inner = device % per_group
     width = zsend.shape[-1]
-    group_rows = zsend.shape[2]
+    group_rows = zsend.shape[1]
     peer_rows = dsend.shape[2]
     slots = GROUPS * group_rows
     rows = per_group * peer_rows
@@ -277,24 +278,35 @@
         other = lax.rem(inner + step, per_group)
         return other, group * per_group + other
 
-    def column_copy(source, target, sems, chunk, step):
+    def send_out(step):
         other, peer = column_peer(step)
         return pltpu.make_async_remote_copy(
-            src_ref=source.at[chunk, other],
-            dst_ref=target.at[chunk, group],
-            send_sem=sems.at[0, chunk, step],
-            recv_sem=sems.at[1, chunk, step],
+            src_ref=zsend.at[other],
+            dst_ref=zrecv.at[step],
+            send_sem=z_sems.at[0, step],
+            recv_sem=z_sems.at[1, step],
             device_id=(peer,),
             device_id_type=MESH,
         )
 
-    def plane_copy(source, target, sems, chunk, step):
+    def send_home(step):
+        home = lax.rem(group + GROUPS - step, GROUPS)
+        return pltpu.make_async_remote_copy(
+            src_ref=csend.at[step],
+            dst_ref=crecv.at[group],
+            send_sem=c_sems.at[0, step],
+            recv_sem=c_sems.at[1, step],
+            device_id=(home * per_group + inner,),
+            device_id_type=MESH,
+        )
+
+    def plane_copy(source, target, sems, stage, step):
         other, peer = plane_peer(step)
         return pltpu.make_async_remote_copy(
-            src_ref=source.at[chunk, other],
-            dst_ref=target.at[chunk, inner],
-            send_sem=sems.at[0, chunk, step],
-            recv_sem=sems.at[1, chunk, step],
+            src_ref=source.at[stage, other],
+            dst_ref=target.at[stage, inner],
+            send_sem=sems.at[0, stage, step],
+            recv_sem=sems.at[1, stage, step],
             device_id=(peer,),
             device_id_type=MESH,
         )
@@ -303,7 +315,7 @@
         other, peer = column_peer(step)
         return pltpu.make_async_remote_copy(
             src_ref=meta_send.at[other],
-            dst_ref=meta_recv.at[group],
+            dst_ref=meta_recv.at[step],
             send_sem=meta_sems.at[0, step],
             recv_sem=meta_sems.at[1, step],
             device_id=(peer,),
@@ -311,7 +323,7 @@
         )
 
     def each_column(act):
-        for step in (2, 1, 3):
+        for step in range(1, GROUPS):
             act(step)
 
     def each_plane(act):
@@ -339,7 +351,8 @@
 
     each_column(greet_column)
     each_plane(greet_plane)
-    seq_count = normed.shape[0]
+    seq_count = mixed.shape[0]
+    normed = rms(mixed[...].astype(jnp.float32), moe_gain[...]).astype(jnp.bfloat16)
     group_row = expert_group[...].astype(jnp.float32)
     inner_rows = [expert_inner[choice : choice + 1, :].astype(jnp.float32) for choice in (0, 1)]
     square = (seq_count, seq_count)
@@ -356,12 +369,10 @@
     group_slot = group_row * group_rows + earlier([column(group_row)], group_row)
     expert_rows = [group_row * per_group + row for row in inner_rows]
     expert_columns = [column(row) for row in expert_rows]
-    capacity = peer_rows // GROUPS
-    own_rows = (group * capacity + 1).astype(jnp.float32)
     lanes = []
     for choice in (0, 1):
         slot = earlier(expert_columns, expert_rows[choice])
-        lanes.append(column(inner_rows[choice] * peer_rows + own_rows + slot))
+        lanes.append(column(inner_rows[choice] * peer_rows + slot + 1.0))
     for choice in (0, 1):
         weight = column(route_weights[choice : choice + 1, :])
         high = weight.astype(jnp.bfloat16).astype(jnp.float32)
@@ -376,96 +387,100 @@
     collecting = (slot_across == column(group_slot)).astype(jnp.float32).astype(jnp.bfloat16)
     meta = dot(placing, token_meta.astype(jnp.bfloat16)).astype(jnp.bfloat16)
     meta_send[...] = meta.reshape(meta_send.shape)
-    for chunk in range(CHUNKS):
-        columns = slice(chunk * width, (chunk + 1) * width)
-        block = dot(placing, normed[:, columns]).astype(jnp.bfloat16)
-        zsend[chunk] = block.reshape(zsend.shape[1:])
+    zsend[...] = dot(placing, normed).astype(jnp.bfloat16).reshape(zsend.shape)
     pl.semaphore_wait(barrier, GROUPS - 1 + per_group - 1)
     each_column(lambda step: meta_copy(step).start())
-    for chunk in range(CHUNKS):
-        each_column(lambda step: column_copy(zsend, zrecv, z_sems, chunk, step).start())
-    meta_recv[group] = meta_send[group]
-    for chunk in range(CHUNKS):
-        zrecv[chunk, group] = zsend[chunk, group]
-    each_column(lambda step: meta_copy(step).wait_recv())
-    meta = meta_recv[...].reshape(slots, meta_recv.shape[-1]).astype(jnp.float32)
-    row_ids = lax.broadcasted_iota(jnp.int32, (slots, rows), 1).astype(jnp.float32) + 1.0
-    first = (row_ids == meta[:, 0:1]).astype(jnp.float32)
-    second = (row_ids == meta[:, 1:2]).astype(jnp.float32)
-    spread = (first + second).astype(jnp.bfloat16)
-    weights = first * (meta[:, 2:3] + meta[:, 3:4]) + second * (meta[:, 4:5] + meta[:, 5:6])
-    weights_high = weights.astype(jnp.bfloat16)
-    weights_low = (weights - weights_high.astype(jnp.float32)).astype(jnp.bfloat16)
-    for chunk in range(CHUNKS):
-        each_column(lambda step: column_copy(zsend, zrecv, z_sems, chunk, step).wait_recv())
+    each_column(lambda step: send_out(step).start())
+    meta_recv[0] = meta_send[group]
+    zrecv[0] = zsend[group]
+    weights_of = {}
+
+    def spread_rows(stage):
+        if stage:
+            meta_copy(stage).wait_recv()
+        meta = meta_recv[stage].astype(jnp.float32)
+        row_ids = lax.broadcasted_iota(jnp.int32, (group_rows, rows), 1).astype(jnp.float32) + 1.0
+        first = (row_ids == meta[:, 0:1]).astype(jnp.float32)
+        second = (row_ids == meta[:, 1:2]).astype(jnp.float32)
+        weights = first * (meta[:, 2:3] + meta[:, 3:4]) + second * (meta[:, 4:5] + meta[:, 5:6])
+        high = weights.astype(jnp.bfloat16)
+        weights_of[stage] = (high, (weights - high.astype(jnp.float32)).astype(jnp.bfloat16))
+        if stage:
+            send_out(stage).wait_recv()
         block = lax.dot_general(
-            spread,
-            zrecv[chunk].reshape(slots, width),
+            (first + second).astype(jnp.bfloat16),
+            zrecv[stage],
             (((0,), (0,)), ((), ())),
             preferred_element_type=jnp.float32,
         ).astype(jnp.bfloat16)
-        dsend[chunk] = block.reshape(dsend.shape[1:])
-        each_plane(lambda step: plane_copy(dsend, drecv, d_sems, chunk, step).start())
-        drecv[chunk, inner] = dsend[chunk, inner]
-    loads[0].wait()
-    loads[1].wait()
-    loads[2].wait()
-    gate_part = jnp.zeros((rows, gate_w.shape[1]), jnp.float32)
-    up_part = jnp.zeros((rows, gate_w.shape[1]), jnp.float32)
-    for chunk in range(CHUNKS):
-        columns = slice(chunk * width, (chunk + 1) * width)
-        each_plane(lambda step: plane_copy(dsend, drecv, d_sems, chunk, step).wait_recv())
-        block = drecv[chunk].reshape(rows, width)
-        gate_part += dot(block, gate_w[columns, :])
-        up_part += dot(block, up_w[columns, :])
-    hidden = (jax.nn.silu(gate_part) * up_part).astype(jnp.bfloat16)
-    for chunk in range(CHUNKS):
-        columns = slice(chunk * width, (chunk + 1) * width)
-        block = dot(hidden, down_w[:, columns]).astype(jnp.bfloat16)
-        osend[chunk] = block.reshape(osend.shape[1:])
-        each_plane(lambda step: plane_copy(osend, orecv, o_sems, chunk, step).start())
-        orecv[chunk, inner] = osend[chunk, inner]
-    for chunk in range(CHUNKS):
-        each_plane(lambda step: plane_copy(osend, orecv, o_sems, chunk, step).wait_recv())
-        block = orecv[chunk].reshape(rows, width)
-        block = (dot(weights_high, block) + dot(weights_low, block)).astype(jnp.bfloat16)
-        csend[chunk] = block.reshape(csend.shape[1:])
-        each_column(lambda step: column_copy(csend, crecv, c_sems, chunk, step).start())
-        crecv[chunk, group] = csend[chunk, group]
-    for chunk in range(CHUNKS):
-        columns = slice(chunk * width, (chunk + 1) * width)
-        each_column(lambda step: column_copy(csend, crecv, c_sems, chunk, step).wait_recv())
-        block = dot(collecting, crecv[chunk].reshape(slots, width))
-        out[:, columns] = (mixed[:, columns].astype(jnp.float32) + block).astype(jnp.bfloat16)
+        dsend[stage] = block.reshape(dsend.shape[1:])
+        each_plane(lambda step: plane_copy(dsend, drecv, d_sems, stage, step).start())
+        drecv[stage, inner] = dsend[stage, inner]
+
+    def run_expert(stage):
+        each_plane(lambda step: plane_copy(dsend, drecv, d_sems, stage, step).wait_recv())
+        if stage == 0:
+            for load in loads:
+                load.wait()
+        block = drecv[stage].reshape(rows, width)
+        hidden = jax.nn.silu(dot(block, gate_w[...])) * dot(block, up_w[...])
+        block = dot(hidden.astype(jnp.bfloat16), down_w[...]).astype(jnp.bfloat16)
+        osend[stage] = block.reshape(osend.shape[1:])
+        each_plane(lambda step: plane_copy(osend, orecv, o_sems, stage, step).start())
+        orecv[stage, inner] = osend[stage, inner]
+
+    def combine(stage):
+        each_plane(lambda step: plane_copy(osend, orecv, o_sems, stage, step).wait_recv())
+        block = orecv[stage].reshape(rows, width)
+        high, low = weights_of[stage]
+        csend[stage] = (dot(high, block) + dot(low, block)).astype(jnp.bfloat16)
+        if stage:
+            send_home(stage).start()
+        else:
+            crecv[group] = csend[0]
+
+    spread_rows(0)
+    spread_rows(1)
+    run_expert(0)
+    spread_rows(2)
+    run_expert(1)
+    spread_rows(3)
+    combine(0)
+    run_expert(2)
+    combine(1)
+    run_expert(3)
+    combine(2)
+    combine(3)
+    each_column(lambda step: send_home(step).wait_recv())
+    block = dot(collecting, crecv[...].reshape(slots, width))
+    out[...] = (mixed[...].astype(jnp.float32) + block).astype(jnp.bfloat16)
     each_column(lambda step: meta_copy(step).wait_send())
-
-    def drain(chunk, carry):
-        each_column(lambda step: column_copy(zsend, zrecv, z_sems, chunk, step).wait_send())
-        each_column(lambda step: column_copy(csend, crecv, c_sems, chunk, step).wait_send())
-        each_plane(lambda step: plane_copy(dsend, drecv, d_sems, chunk, step).wait_send())
-        each_plane(lambda step: plane_copy(osend, orecv, o_sems, chunk, step).wait_send())
+    each_column(lambda step: send_out(step).wait_send())
+    each_column(lambda step: send_home(step).wait_send())
+
+    def drain(stage, carry):
+        each_plane(lambda step: plane_copy(dsend, drecv, d_sems, stage, step).wait_send())
+        each_plane(lambda step: plane_copy(osend, orecv, o_sems, stage, step).wait_send())
         return carry
 
-    lax.fori_loop(0, CHUNKS, drain, 0)
+    lax.fori_loop(0, STAGES, drain, 0)
 
 
 def routed_experts(
-    mixed_tokens, normed_moe, route_weights, expert_group, expert_inner, expert_gate, expert_up, expert_down
+    mixed_tokens, moe_gain, route_weights, expert_group, expert_inner, expert_gate, expert_up, expert_down
 ):
     experts = lax.axis_size("ep")
     per_group = experts // GROUPS
-    seq_count, model_width = normed_moe.shape
+    seq_count, model_width = mixed_tokens.shape
     capacity = max(2, 4 * seq_count // experts)
     group_rows = -(-min(seq_count, per_group * capacity // TOP_K) // 8) * 8
-    peer_rows = GROUPS * capacity
-    width = model_width // CHUNKS
+    peer_rows = -(-capacity // 8) * 8
     hidden_width = expert_gate.shape[-1]
-    slots = GROUPS * group_rows
     vmem = pl.BlockSpec(memory_space=pltpu.VMEM)
     hbm = pl.BlockSpec(memory_space=pl.ANY)
     bf16 = jnp.bfloat16
-    column_buffer = pltpu.VMEM((CHUNKS, GROUPS, group_rows, width), bf16)
-    plane_buffer = pltpu.VMEM((CHUNKS, per_group, peer_rows, width), bf16)
+    column_buffer = pltpu.VMEM((GROUPS, group_rows, model_width), bf16)
+    plane_buffer = pltpu.VMEM((STAGES, per_group, peer_rows, model_width), bf16)
     meta_buffer = pltpu.VMEM((GROUPS, group_rows, 128), bf16)
     dma = pltpu.SemaphoreType.DMA
 
@@ -494,16 +509,18 @@
             column_buffer,
             dma((3,)),
             dma((2, GROUPS)),
-            dma((2, CHUNKS, GROUPS)),
-            dma((2, CHUNKS, per_group)),
-            dma((2, CHUNKS, per_group)),
-            dma((2, CHUNKS, GROUPS)),
+            dma((2, STAGES)),
+            dma((2, STAGES, per_group)),
+            dma((2, STAGES, per_group)),
+            dma((2, STAGES)),
         ],
         compiler_params=pltpu.CompilerParams(
-            collective_id=0, has_side_effects=True, vmem_limit_bytes=60 * 1024 * 1024
+            collective_id=0,
+            has_side_effects=True,
+            vmem_limit_bytes=(16 + 20 * per_group // 32 * 2) * 1024 * 1024,
         ),
     )(
-        normed_moe,
+        moe_gain.reshape(1, -1),
         mixed_tokens,
         expert_group.reshape(1, -1),
         expert_inner.T,
@@ -534,7 +551,7 @@
     expert_up,
     expert_down,
 ):
-    mixed_tokens, normed_moe, new_state = retention_step(
+    mixed_tokens, new_state = retention_step(
         tokens,
         history_length,
         norm_gain,
@@ -546,11 +563,10 @@
         state,
         head_gain,
         w_out,
-        moe_gain,
     )
     output = routed_experts(
         mixed_tokens,
-        normed_moe,
+        moe_gain,
         route_weights,
         expert_group,
         expert_inner,

time: 60.5 us -> 58.9 us (0.974)
  other arithmetic: 1.47 us -> 0 us
    sin x1 -> x0, other arithmetic: 0.8 us -> none  [retention_step(): jnp.sin(angles)]
    convert_element_type x1 -> x0, other arithmetic: 0.66 us -> none  [retention_step(): angles = history_length.astype(jnp.float32)[:, None] * inverse[None, :]]
    unnamed x1 -> x17, local copies, waits for them, and re-layouts: 1.62 us -> 1.63 us
where the time goes in v3:
time: 58.9 us; the launch traced here: 58.8 us
  Pallas kernels  56.4 us (96%)
  local copies, waits for them, and re-layouts  1.63 us (3%)
  between operations  0.77 us (1%)
    pallas_call x1, Pallas kernels, routed_experts(): pl.pallas_call(kernel, name='experts', out_shape=jax.ShapeDtypeStruct((se...  40.3 us
    pallas_call x1, Pallas kernels, retention_step(): pl.pallas_call(retention_kernel, name='retention', out_shape=(row_shape,...  16.1 us
    unnamed x17, local copies, waits for them, and re-layouts  1.63 us

profile of v3, /device:TPU:0, one launch (start us, length us, event | category | flops | bytes accessed | tf_op | source)
XLA Modules:
  0.0 58.8 jit_solution(18323207379902139247)
XLA Ops:
  0.6 0.0 copy-start
  0.6 0.0 copy-start.1
  0.7 0.0 copy-start.2
  0.7 0.0 copy-start.4
  0.7 0.0 copy-start.5
  0.7 0.0 copy-start.6
  0.7 0.0 copy-start.7
  0.7 16.1 %retention.1 = (bf16[48,2048]{1,0:T(8,128)(2,1)}, f32[48,8,64,64]{3,2,1,0:T(8,128)}) custom-call(bf16[48,2048]{1,0:T(8,128)(2,1)} %tokens.1, s32[1,48]{1,0:T(1,128)} %bitcast.19, f32[1,32]{1,0:T(1,128)} %constant.2.clone.inverse, f32[1,2048]{1,0:T(1,128)} %bitcast.17, f32[8]{0:T(128)} %decay_rate.1, f32[1,512]{1,0:T(1,128)} %bitcast.18, ...), custom_call_target="tpu_custom_call" | custom-call | tf_op jit(solution)/shard_map/retention/pallas_call | solution.py:194
  16.8 0.0 copy-done
  16.8 0.0 copy-done.1
  16.8 0.0 copy-done.2
  16.8 0.0 copy-done.4
  16.8 0.0 copy-done.5
  16.8 0.0 copy-done.6
  16.9 0.0 copy-done.7
  16.9 0.0 copy-start.3
  16.9 0.9 %copy-done.3 = bf16[48,2048]{1,0:T(8,128)(2,1)S(1)} copy-done((bf16[48,2048]{1,0:T(8,128)(2,1)S(1)}, bf16[48,2048]{1,0:T(8,128)(2,1)}, u32[]{:S(2)}) %copy-start.3) | copy-done | bytes 196632
  17.8 40.3 %experts.1 = bf16[48,2048]{1,0:T(8,128)(2,1)S(1)} custom-call(f32[1,2048]{1,0:T(1,128)S(1)} %bitcast.13, bf16[48,2048]{1,0:T(8,128)(2,1)S(1)} %copy-done.3, s32[1,48]{1,0:T(1,128)S(1)} %bitcast.16, s32[2,48]{1,0:T(2,128)S(1)} %bitcast.14, f32[2,48]{1,0:T(2,128)S(1)} %bitcast.15, bf16[2048,256]{1,0:T(8,128)(2,1)S(1)} %bitcast.10, ...), custom_call_target="tpu_custom_call" | custom-call | tf_op jit(solution)/shard_map/experts/pallas_call | solution.py:490
  58.1 0.7 %copy.22 = bf16[48,2048]{1,0:T(8,128)(2,1)} copy(bf16[48,2048]{1,0:T(8,128)(2,1)S(1)} %experts.1) | data formatting | bytes 393216
Async XLA Ops:
  0.6 16.2 %copy-start = (bf16[1,2048,256]{2,1,0:T(8,128)(2,1)S(1)}, bf16[1,2048,256]{2,1,0:T(8,128)(2,1)}, u32[]{:S(2)}) copy-start(bf16[1,2048,256]{2,1,0:T(8,128)(2,1)} %param.34) | copy-start | bytes 3145732
  0.6 16.2 %copy-start.1 = (bf16[1,2048,256]{2,1,0:T(8,128)(2,1)S(1)}, bf16[1,2048,256]{2,1,0:T(8,128)(2,1)}, u32[]{:S(2)}) copy-start(bf16[1,2048,256]{2,1,0:T(8,128)(2,1)} %param.35) | copy-start | bytes 3145732
  0.7 16.2 %copy-start.2 = (bf16[1,256,2048]{2,1,0:T(8,128)(2,1)S(1)}, bf16[1,256,2048]{2,1,0:T(8,128)(2,1)}, u32[]{:S(2)}) copy-start(bf16[1,256,2048]{2,1,0:T(8,128)(2,1)} %param.36) | copy-start | bytes 3145732
  0.7 16.2 %copy-start.4 = (f32[2048]{0:T(1024)S(1)}, f32[2048]{0:T(1024)}, u32[]{:S(2)}) copy-start(f32[2048]{0:T(1024)} %param.30) | copy-start | bytes 24580
  0.7 16.2 %copy-start.5 = (s32[48,2]{0,1:T(2,128)S(1)}, s32[48,2]{0,1:T(2,128)}, u32[]{:S(2)}) copy-start(s32[48,2]{0,1:T(2,128)} %param.33) | copy-start | bytes 1156
  0.7 16.2 %copy-start.6 = (f32[48,2]{0,1:T(2,128)S(1)}, f32[48,2]{0,1:T(2,128)}, u32[]{:S(2)}) copy-start(f32[48,2]{0,1:T(2,128)} %param.31) | copy-start | bytes 1156
  0.7 16.2 %copy-start.7 = (s32[48]{0:T(128)S(1)}, s32[48]{0:T(128)}, u32[]{:S(2)}) copy-start(s32[48]{0:T(128)} %param.32) | copy-start | bytes 580
  16.9 0.9 %copy-start.3 = (bf16[48,2048]{1,0:T(8,128)(2,1)S(1)}, bf16[48,2048]{1,0:T(8,128)(2,1)}, u32[]{:S(2)}) copy-start(bf16[48,2048]{1,0:T(8,128)(2,1)} %get-tuple-element.4.refs_1_) | copy-start | bytes 589828
